TPU v7x, 1024 devices: a whole 4x4x32 slice. The times are simulated.
1024 devices in a mesh: fs: 128 (over z, y), tp: 8 (over x, core).
Axes of the slice: x: 4, y: 4, z: 32, core: 2. Of those that a mesh axis runs over, the one named last changes fastest.
Arguments:
- tokens: bfloat16 [49152, 2048], P('fs'), may hold values from -6 to 6
- first_norm_scale: float32 [2048], replicated, may hold values from 0.1 to 1.9
- recurrent_branch_matrix: bfloat16 [2048, 1024], P('fs', 'tp'), may hold values from -0.125 to 0.125
- gelu_gate_matrix: bfloat16 [2048, 1024], P('fs', 'tp'), may hold values from -0.125 to 0.125
- filter_taps_weight: bfloat16 [4, 1024], P(None, 'tp'), may hold values from -3 to 3
- recurrence_gate_blocks: bfloat16 [16, 64, 64], P('tp'), may hold values from -0.75 to 0.75
- input_gate_blocks: bfloat16 [16, 64, 64], P('tp'), may hold values from -0.75 to 0.75
- base_decay_logits: float32 [1024], P('tp'), may hold values from 4 to 11
- extra_log_decay: float32 [49152, 1024], P('fs', 'tp'), may hold values from -0.7 to 0
- mixer_output_matrix: bfloat16 [2048, 1024], P('fs', 'tp'), may hold values from -0.5 to 0.5
- second_norm_scale: float32 [2048], replicated, may hold values from 0.1 to 1.9
- mixer_up_matrix: bfloat16 [2048, 4096], P('fs', 'tp'), may hold values from -0.125 to 0.125
- mixer_down_matrix: bfloat16 [2048, 4096], P('fs', 'tp'), may hold values from -0.09375 to 0.09375
Outputs:
- layer_out: bfloat16 [49152, 2048], P(('fs', 'tp'))
All inputs are finite; a program needn't handle non-finite values.
Results may differ from a plain program's by a relative error of at most 0.022.
Values may be sent and summed in bfloat16 or wider, within the bound.
No kernel may reach another device: no remote copies, remote signals or barrier semaphores. Data moves between devices by JAX's collectives and lax.ppermute only.
A program may use at most 32 MiB of HBM per device.

v0:
```python
import jax
import jax.numpy as jnp
from jax import lax
from jax.sharding import PartitionSpec as P

epsilon = 1e-06
decay_rate_scale = 8.0


def side_by_side(arrays, axis, dim, along):
    widths = [a.shape[along] for a in arrays]
    both = jnp.concatenate(arrays, axis=along)
    whole = lax.all_gather(both, axis, axis=dim, tiled=True)
    return tuple(jnp.split(whole, [sum(widths[:k]) for k in range(1, len(widths))], axis=along))


def in_blocks(array, dim, count):
    shape = array.shape
    tiles = array.reshape(*shape[:dim], count, shape[dim] // count, *shape[dim + 1 :])
    return jnp.moveaxis(tiles, dim, 0)


def sent_and_summed(array, axis, dim):
    tiles = in_blocks(array, dim, lax.axis_size(axis))
    arrived = lax.all_to_all(tiles, axis, split_axis=0, concat_axis=0, tiled=True)
    return arrived.astype(jnp.float32).sum(axis=0)


def from_everyone(array, axis):
    count = lax.axis_size(axis)
    return lax.all_to_all(
        jnp.broadcast_to(array[None], (count, *array.shape)), axis, 0, 0, tiled=True
    )


def laid_out(tiles, dim):
    shape = list(tiles.shape[1:])
    shape[dim] *= tiles.shape[0]
    return jnp.moveaxis(tiles, 0, dim).reshape(shape)


def gather_directly(array, axis, dim):
    tiles = from_everyone(array, axis)
    return laid_out(tiles, dim)


def rms_scaled(sequence_token_rows, scales):
    widened = sequence_token_rows.astype(jnp.float32)
    mean_square = jnp.mean(widened * widened, axis=-1, keepdims=True)
    return (widened * lax.rsqrt(mean_square + epsilon) * scales).astype(jnp.bfloat16)


def linear_combine(earlier, later):
    return (earlier[0] * later[0], later[0] * earlier[1] + later[1])


def causal_taps(branch, filter_taps_weight):
    tap_count = filter_taps_weight.shape[0]
    positions = branch.shape[0]
    padded = jnp.pad(branch.astype(jnp.float32), ((tap_count - 1, 0), (0, 0)))
    running = jnp.zeros(branch.shape, jnp.float32)
    for offset in range(tap_count):
        running = running + padded[offset : offset + positions] * filter_taps_weight[offset].astype(
            jnp.float32
        )
    return running.astype(jnp.bfloat16)


def block_map(convolved, blocks):
    positions, channels = convolved.shape
    grouped = convolved.reshape(positions, blocks.shape[0], blocks.shape[1])
    mapped = jnp.einsum("sgi,gij->sgj", grouped, blocks, preferred_element_type=jnp.float32)
    return jax.nn.sigmoid(mapped.reshape(positions, channels))


def contract_columns(left, right):
    return lax.dot_general(
        left, right, (((1,), (1,)), ((), ())), preferred_element_type=jnp.float32
    )


def local(
    tokens,
    first_norm_scale,
    recurrent_branch_matrix,
    gelu_gate_matrix,
    filter_taps_weight,
    recurrence_gate_blocks,
    input_gate_blocks,
    base_decay_logits,
    extra_log_decay,
    mixer_output_matrix,
    second_norm_scale,
    mixer_up_matrix,
    mixer_down_matrix,
):
    positions = tokens.shape[0]
    own_count = positions // lax.axis_size("tp")
    normed = rms_scaled(tokens, first_norm_scale)
    branch_full, gate_full, out_full, up_full, down_full = side_by_side(
        (
            recurrent_branch_matrix,
            gelu_gate_matrix,
            mixer_output_matrix,
            mixer_up_matrix,
            mixer_down_matrix,
        ),
        "fs",
        0,
        1,
    )
    branch = jnp.dot(normed, branch_full, preferred_element_type=jnp.float32).astype(jnp.bfloat16)
    gate_branch = jnp.dot(normed, gate_full, preferred_element_type=jnp.float32).astype(
        jnp.bfloat16
    )
    convolved = causal_taps(branch, filter_taps_weight)
    recurrence_gate_value = block_map(convolved, recurrence_gate_blocks)
    admission = block_map(convolved, input_gate_blocks)
    log_keep_factor = (
        decay_rate_scale * recurrence_gate_value * jax.nn.log_sigmoid(base_decay_logits)
        + extra_log_decay
    )
    retain = jnp.exp(log_keep_factor)
    driven = jnp.sqrt(-jnp.expm1(2.0 * log_keep_factor)) * (
        admission * convolved.astype(jnp.float32)
    )
    memory = lax.associative_scan(linear_combine, (retain, driven), axis=0)[1]
    recurrent = (memory * jax.nn.gelu(gate_branch.astype(jnp.float32))).astype(jnp.bfloat16)
    picked = recurrent
    mixer_out = sent_and_summed(contract_columns(picked, out_full).astype(jnp.bfloat16), "tp", 0)
    own_rows = lax.dynamic_slice_in_dim(tokens, lax.axis_index("tp") * own_count, own_count, 0)
    residual = (own_rows.astype(jnp.float32) + mixer_out).astype(jnp.bfloat16)
    normed_mid = rms_scaled(residual, second_norm_scale)
    raised = jnp.dot(
        gather_directly(normed_mid, "tp", 0), up_full, preferred_element_type=jnp.float32
    )
    hidden = jnp.square(jax.nn.relu(raised)).astype(jnp.bfloat16)
    picked = hidden
    channel_sum = sent_and_summed(contract_columns(picked, down_full).astype(jnp.bfloat16), "tp", 0)
    return (residual.astype(jnp.float32) + channel_sum).astype(jnp.bfloat16)


def solution(mesh):
    in_specs = (
        P("fs", None),
        P(),
        P("fs", "tp"),
        P("fs", "tp"),
        P(None, "tp"),
        P("tp", None, None),
        P("tp", None, None),
        P("tp"),
        P("fs", "tp"),
        P("fs", "tp"),
        P(),
        P("fs", "tp"),
        P("fs", "tp"),
    )
    out_specs = P(("fs", "tp"), None)
    return jax.shard_map(local, mesh=mesh, in_specs=in_specs, out_specs=out_specs, check_vma=False)
```

profile of v0, /device:TPU:1, one launch (start us, length us, event | category | flops | bytes accessed | tf_op | source)
XLA Modules:
  0.0 392.8 jit_solution(14566290826518664738)
XLA Ops:
  6.5 0.0 copy-start
  6.5 0.0 all-gather.2.cloned.1.call-start
  6.5 0.7 constant_dynamic-update-slice_fusion.4
  7.2 0.7 constant_dynamic-update-slice_fusion.3
  7.9 0.7 constant_dynamic-update-slice_fusion.2
  8.6 0.7 constant_dynamic-update-slice_fusion.1
  9.3 0.7 constant_dynamic-update-slice_fusion
  10.1 0.0 copy-start.3
  10.1 0.6 copy-done.3
  10.7 0.0 all-gather.2.cloned.1.call-update
  10.7 1.8 fusion
  12.5 0.7 fusion.73
  13.2 0.8 bitcast_convert_fusion.3
  14.0 0.0 copy-start.5
  14.0 264.8 %all-gather.2.cloned.1.call-done = bf16[2048,1408]{1,0:T(8,128)(2,1)} async-done(((bf16[16,1408]{1,0:T(8,128)(2,1)}), bf16[2048,1408]{1,0:T(8,128)(2,1)}) %all-gather.2.cloned.1.call-update) | async-done | bytes 5767184 | tf_op jit(solution)/shard_map/all_gather | solution.py:13
  278.8 2.2 fusion.22
  281.0 0.0 copy-start.2
  281.0 0.1 add_convert_fusion.1
  281.1 0.1 copy.20
  281.2 0.0 copy-done
  281.2 0.2 fusion.17
  281.5 0.1 copy.24
  281.6 0.0 copy-done.5
  281.6 0.2 fusion.20
  281.9 0.1 copy.22
  282.0 0.0 copy-done.2
  282.0 0.2 fusion.67
  282.6 0.0 copy-start.1
  282.6 0.0 copy-start.6
  283.8 0.2 copy-done.1
  284.0 0.0 copy-done.6
  284.0 4.2 %convolution_convert_fusion.1 = bf16[384,2048]{1,0:T(8,128)(2,1)} fusion(bf16[2048,1408]{1,0:T(8,128)(2,1)} %all-gather.2.cloned.1.call-done, bf16[384,2048]{1,0:T(8,128)(2,1)S(1)} %copy-done.1, f32[2048]{0:T(1024)S(1)} %copy-done.6, f32[384]{0:T(512)S(1)} %add_rsqrt_fusion, f32[384,128]{1,0:T(8,128)S(1)} %pad.68, f32[384,128]{1,0:T(8,128)S(1)} %pad.69), kind=kOutput, calls=%fused_computation.8 | convolution fusion | flops 407224320 | bytes 4597248 | tf_op jit(solution)/shard_map/dot_general | solution.py:77
  288.3 23.4 %all-to-all-start = ((bf16[8,48,2048]{2,1,0:T(8,128)(2,1)}), bf16[8,48,2048]{2,1,0:T(8,128)(2,1)S(1)}, u32[]{:S(2)}, u32[]{:S(2)}) async-start(bf16[8,48,2048]{2,1,0:T(8,128)(2,1)} %bitcast.27), calls=%async_computation | async-start | bytes 3145728 | tf_op jit(solution)/shard_map/all_to_all | solution.py:25
  311.7 0.0 copy-start.4
  311.7 20.6 %all-to-all-done = bf16[8,48,2048]{2,1,0:T(8,128)(2,1)S(1)} async-done(((bf16[8,48,2048]{2,1,0:T(8,128)(2,1)}), bf16[8,48,2048]{2,1,0:T(8,128)(2,1)S(1)}, u32[]{:S(2)}, u32[]{:S(2)}) %all-to-all-start) | async-done | bytes 1572896 | tf_op jit(solution)/shard_map/all_to_all | solution.py:25
  332.3 0.2 convert_reduce_fusion.1
  332.5 0.2 fusion.30
  332.7 0.0 copy-done.4
  332.7 0.1 fusion.32
  332.8 0.2 broadcast_in_dim.2
  333.0 24.0 %all_to_all.15 = bf16[8,48,2048]{2,1,0:T(8,128)(2,1)S(1)} all-to-all(bf16[8,48,2048]{2,1,0:T(8,128)(2,1)S(1)} %broadcast_in_dim.2), channel_id=1, replica_groups=mesh['fs'=128,'tp'=8] {'tp'}, dimensions={0} | all-to-all | bytes 3145728 | tf_op jit(solution)/shard_map/all_to_all | solution.py:31
  356.9 4.1 %convolution_convert_fusion = bf16[384,2048]{1,0:T(8,128)(2,1)S(1)} fusion(bf16[2048,1408]{1,0:T(8,128)(2,1)} %all-gather.2.cloned.1.call-done, bf16[384,2048]{1,0:T(8,128)(2,1)S(1)} %bitcast.28), kind=kOutput, calls=%fused_computation.7 | convolution fusion | flops 1611988992 | bytes 7340032 | tf_op jit(solution)/shard_map/dot_general | solution.py:77
  361.0 24.0 %all_to_all.16 = bf16[8,48,2048]{2,1,0:T(8,128)(2,1)S(1)} all-to-all(bf16[8,48,2048]{2,1,0:T(8,128)(2,1)S(1)} %bitcast.29), channel_id=1, replica_groups=mesh['fs'=128,'tp'=8] {'tp'}, dimensions={0} | all-to-all | bytes 3145728 | tf_op jit(solution)/shard_map/all_to_all | solution.py:25
  385.0 0.2 convert_reduce_fusion
  385.3 0.7 fusion.33
  (96 shorter events, 1.1 us)
Async XLA Ops:
  6.5 274.7 %copy-start = (bf16[2,64,64]{2,1,0:T(8,128)(2,1)S(1)}, bf16[2,64,64]{2,1,0:T(8,128)(2,1)}, u32[]{:S(2)}) copy-start(bf16[2,64,64]{2,1,0:T(8,128)(2,1)} %param.19) | copy-start | bytes 49156
  6.5 272.3 %all-gather.2.cloned.1.call-start = ((), (), s32[]{:S(2)}) async-start(), calls=%async_computation.3 | async-start | bytes 5812224 | tf_op jit(solution)/shard_map/all_gather | solution.py:13
  10.1 0.6 copy-start.3
  14.0 267.6 %copy-start.5 = (bf16[2,64,64]{2,1,0:T(8,128)(2,1)S(1)}, bf16[2,64,64]{2,1,0:T(8,128)(2,1)}, u32[]{:S(2)}) copy-start(bf16[2,64,64]{2,1,0:T(8,128)(2,1)} %param.18) | copy-start | bytes 49156
  281.0 1.0 copy-start.2
  282.6 1.4 copy-start.1
  282.6 1.4 copy-start.6
  288.3 44.0 %all-to-all-start = ((bf16[8,48,2048]{2,1,0:T(8,128)(2,1)}), bf16[8,48,2048]{2,1,0:T(8,128)(2,1)S(1)}, u32[]{:S(2)}, u32[]{:S(2)}) async-start(bf16[8,48,2048]{2,1,0:T(8,128)(2,1)} %bitcast.27), calls=%async_computation | async-start | bytes 3145728 | tf_op jit(solution)/shard_map/all_to_all | solution.py:25
  311.7 21.0 %copy-start.4 = (f32[2048]{0:T(1024)S(1)}, f32[2048]{0:T(1024)}, u32[]{:S(2)}) copy-start(f32[2048]{0:T(1024)} %param.23) | copy-start | bytes 24580
Sparse Core Ops, SparseCore 0:
  11.5 267.2 all-gather.1
where the time goes:
time: 393 us
  waiting for transfers between devices  285 us (73%)
  blocking collectives  48 us (12%)
  starting transfers between devices  23.4 us (6%)
  between operations  14 us (4%)
  matrix products  11 us (3%)
  local copies, waits for them, and re-layouts  5.74 us (1%)
  other arithmetic  5.42 us (1%)
    all_gather x1, waiting for transfers between devices, side_by_side(): whole = lax.all_gather(both, axis, axis=dim, tiled=True)  265 us
    all_to_all x1, blocking collectives, sent_and_summed(): lax.all_to_all(tiles, axis, split_axis=0, concat_axis=0, tiled=True)  24 us
    all_to_all x1, blocking collectives, from_everyone(): lax.all_to_all(jnp.broadcast_to(array[None], (count, *array.shape)), axis...  24 us
    all_to_all x1, starting transfers between devices, sent_and_summed(): lax.all_to_all(tiles, axis, split_axis=0, concat_axis=0, tiled=True)  23.4 us
    all_to_all x1, waiting for transfers between devices, sent_and_summed(): lax.all_to_all(tiles, axis, split_axis=0, concat_axis=0, tiled=True)  20.6 us
    dot_general x2, matrix products, contract_columns(): lax.dot_general(left, right, (((1,), (1,)), ((), ())), preferred_element_...  8.31 us
  transfers between devices with their start and end apart: 2, of which 2 were waited for; matrix products, arithmetic and copies ran while one was open for 1% of the time, Pallas kernels for 0%

commit v1 on v0

v1 whole, which is shorter than its diff:
```python
import jax
import jax.numpy as jnp
from jax import lax
from jax.sharding import Mesh, PartitionSpec as P

epsilon = 1e-06
decay_rate_scale = 8.0
wire_scale = 65536.0


def ring(count, step):
    return [(k, (k + step) % count) for k in range(count)]


def rms_scaled(rows, scales):
    widened = rows.astype(jnp.float32)
    mean_square = jnp.mean(widened * widened, axis=-1, keepdims=True)
    return (widened * lax.rsqrt(mean_square + epsilon) * scales).astype(jnp.bfloat16)


def linear_combine(earlier, later):
    return (earlier[0] * later[0], later[0] * earlier[1] + later[1])


def causal_taps(branch, filter_taps_weight):
    tap_count = filter_taps_weight.shape[0]
    positions = branch.shape[0]
    padded = jnp.pad(branch.astype(jnp.float32), ((tap_count - 1, 0), (0, 0)))
    running = jnp.zeros(branch.shape, jnp.float32)
    for offset in range(tap_count):
        running = running + padded[offset : offset + positions] * filter_taps_weight[offset].astype(
            jnp.float32
        )
    return running.astype(jnp.bfloat16)


def block_map(convolved, blocks):
    positions, channels = convolved.shape
    grouped = convolved.reshape(positions, blocks.shape[0], blocks.shape[1])
    mapped = jnp.einsum("sgi,gij->sgj", grouped, blocks, preferred_element_type=jnp.float32)
    return jax.nn.sigmoid(mapped.reshape(positions, channels))


def contract_columns(left, right):
    return lax.dot_general(
        left, right, (((1,), (1,)), ((), ())), preferred_element_type=jnp.float32
    )


def y_pieces(rows):
    count = lax.axis_size("y")
    pieces = [rows]
    for step in (1, count - 1, 2):
        pieces.append(lax.ppermute(rows, "y", ring(count, step)))
    return pieces


def placed(pieces, z_count):
    count = len(pieces)
    height, width = pieces[0].shape
    me = lax.axis_index("y")
    whole = jnp.zeros((z_count, count, height // z_count, width), pieces[0].dtype)
    for step, piece in zip((0, 1, count - 1, 2), pieces):
        origin = lax.rem(me + count - step, count)
        tiles = piece.reshape(z_count, 1, height // z_count, width)
        whole = lax.dynamic_update_slice_in_dim(whole, tiles, origin, 1)
    return whole.reshape(count * height, width)


def x_summed(rows):
    count = lax.axis_size("x")
    tiles = rows.reshape(count, rows.shape[0] // count, rows.shape[1])
    arrived = lax.all_to_all(tiles, "x", 0, 0, tiled=True)
    return arrived.astype(jnp.float32).sum(axis=0)


def added(left, right):
    return (left.astype(jnp.float32) + right.astype(jnp.float32)).astype(jnp.bfloat16)


def layer(
    tokens,
    first_norm_scale,
    recurrent_branch_matrix,
    gelu_gate_matrix,
    filter_taps_weight,
    recurrence_gate_blocks,
    input_gate_blocks,
    base_decay_logits,
    extra_log_decay,
    mixer_output_matrix,
    second_norm_scale,
    mixer_up_matrix,
    mixer_down_matrix,
):
    positions, _ = tokens.shape
    z_count, x_count, c_count = (lax.axis_size(k) for k in ("z", "x", "c"))
    own_count = positions // (x_count * c_count)
    x_index, c_index = lax.axis_index("x"), lax.axis_index("c")
    channels = recurrent_branch_matrix.shape[1]

    shards = jnp.concatenate(
        [
            recurrent_branch_matrix,
            gelu_gate_matrix,
            mixer_output_matrix,
            mixer_up_matrix,
            mixer_down_matrix,
        ],
        axis=1,
    )
    sent = (shards.astype(jnp.float32) * wire_scale).astype(jnp.float16)
    z_rows = lax.all_gather(sent, "z", axis=0, tiled=True)
    z_rows = (z_rows.astype(jnp.float32) * (1.0 / wire_scale)).astype(jnp.bfloat16)
    first_pieces = y_pieces(z_rows[:, : 3 * channels])
    second_pieces = y_pieces(z_rows[:, 3 * channels :])
    first = placed(first_pieces, z_count)
    second = placed(second_pieces, z_count)
    branch_full, gate_full, out_full = jnp.split(first, 3, axis=1)
    up_full, down_full = jnp.split(second, 2, axis=1)

    normed = rms_scaled(tokens, first_norm_scale)
    branch = jnp.dot(normed, branch_full, preferred_element_type=jnp.float32).astype(jnp.bfloat16)
    gate_branch = jnp.dot(normed, gate_full, preferred_element_type=jnp.float32).astype(
        jnp.bfloat16
    )
    convolved = causal_taps(branch, filter_taps_weight)
    rate = block_map(convolved, recurrence_gate_blocks)
    admission = block_map(convolved, input_gate_blocks)
    log_keep = decay_rate_scale * rate * jax.nn.log_sigmoid(base_decay_logits) + extra_log_decay
    retain = jnp.exp(log_keep)
    driven = jnp.sqrt(-jnp.expm1(2.0 * log_keep)) * (admission * convolved.astype(jnp.float32))
    memory = lax.associative_scan(linear_combine, (retain, driven), axis=0)[1]
    recurrent = (memory * jax.nn.gelu(gate_branch.astype(jnp.float32))).astype(jnp.bfloat16)

    by_core = recurrent.reshape(x_count, c_count, own_count, channels)

    def rows_of(core):
        return lax.dynamic_index_in_dim(by_core, core, 1, keepdims=False).reshape(-1, channels)

    given = contract_columns(rows_of(1 - c_index), out_full).astype(jnp.bfloat16)
    kept = contract_columns(rows_of(c_index), out_full).astype(jnp.bfloat16)
    mixer_out = x_summed(added(kept, lax.ppermute(given, "c", ring(c_count, 1))))
    own_rows = lax.dynamic_slice_in_dim(
        tokens, (x_index * c_count + c_index) * own_count, own_count, 0
    )
    residual = (own_rows.astype(jnp.float32) + mixer_out).astype(jnp.bfloat16)
    normed_mid = rms_scaled(residual, second_norm_scale)

    mine = lax.all_gather(normed_mid, "x", axis=0, tiled=True)
    other = lax.ppermute(mine, "c", ring(c_count, 1))

    def mixed(rows):
        raised = jnp.dot(rows, up_full, preferred_element_type=jnp.float32)
        hidden = jnp.square(jax.nn.relu(raised)).astype(jnp.bfloat16)
        return contract_columns(hidden, down_full).astype(jnp.bfloat16)

    given = mixed(other)
    kept = mixed(mine)
    channel_sum = x_summed(added(kept, lax.ppermute(given, "c", ring(c_count, 1))))
    return (residual.astype(jnp.float32) + channel_sum).astype(jnp.bfloat16)


def solution(mesh):
    z_count = 32 if mesh.shape["fs"] == 128 else mesh.shape["fs"] // 4
    split = Mesh(
        mesh.devices.reshape(z_count, mesh.shape["fs"] // z_count, mesh.shape["tp"] // 2, 2),
        ("z", "y", "x", "c"),
    )
    fs, tp = ("z", "y"), ("x", "c")
    in_specs = (
        P(fs, None),
        P(),
        P(fs, tp),
        P(fs, tp),
        P(None, tp),
        P(tp, None, None),
        P(tp, None, None),
        P(tp),
        P(fs, tp),
        P(fs, tp),
        P(),
        P(fs, tp),
        P(fs, tp),
    )
    return jax.shard_map(
        layer, mesh=split, in_specs=in_specs, out_specs=P((*fs, *tp), None), check_vma=False
    )
```

time: 393 us -> 270 us (0.69)
  waiting for transfers between devices: 285 us -> 21.4 us
  local copies, waits for them, and re-layouts: 5.74 us -> 66.6 us
  blocking collectives: 48 us -> 90.9 us
  starting transfers between devices: 23.4 us -> 53.4 us
  other arithmetic: 5.42 us -> 21.7 us
  between operations: 14 us -> 0.61 us
    all_gather x1 -> x0, waiting for transfers between devices: 265 us -> none  [side_by_side(): whole = lax.all_gather(both, axis, axis=dim, tiled=True)]
    all_gather x0 -> x2, blocking collectives: none -> 75.4 us  [the longest x1 63.7 us: layer(): z_rows = lax.all_gather(sent, 'z', axis=0, tiled=True)]
    ppermute x0 -> x9, starting transfers between devices: none -> 49.4 us  [the longest x2 23.6 us: layer(): lax.ppermute(given, 'c', ring(c_count, 1))]
    slice x49 -> x51, local copies, waits for them, and re-layouts: 0.68 us -> 46.1 us  [the longest x49 46 us: layer(): memory = lax.associative_scan(linear_combine, (retain, driven), axis=0)[1]]
    all_to_all x2 -> x1, blocking collectives: 48 us -> 15.5 us  [x_summed(): arrived = lax.all_to_all(tiles, 'x', 0, 0, tiled=True)]
    ppermute x0 -> x9, waiting for transfers between devices: none -> 19.5 us  [the longest x6 15.8 us: y_pieces(): pieces.append(lax.ppermute(rows, 'y', ring(count, step)))]
    all_to_all x1, starting transfers between devices: 23.4 us -> 4 us  [x_summed(): arrived = lax.all_to_all(tiles, 'x', 0, 0, tiled=True)]
    all_to_all x1, waiting for transfers between devices: 20.6 us -> 1.81 us  [x_summed(): arrived = lax.all_to_all(tiles, 'x', 0, 0, tiled=True)]
  transfers between devices with their start and end apart: 2 -> 10, of which waited for: 2 -> 5; matrix products, arithmetic and copies ran while one was open for 1% -> 6% of each run, Pallas kernels for 0% -> 0%
where the time goes in v1:
time: 270 us; the launch traced here: 266 us
  blocking collectives  90.9 us (34%)
  local copies, waits for them, and re-layouts  66.6 us (25%)
  starting transfers between devices  53.4 us (20%)
  other arithmetic  21.7 us (8%)
  waiting for transfers between devices  21.4 us (8%)
  matrix products  11.9 us (4%)
    all_gather x1, blocking collectives, layer(): z_rows = lax.all_gather(sent, 'z', axis=0, tiled=True)  63.7 us
    slice x49, local copies, waits for them, and re-layouts, layer(): memory = lax.associative_scan(linear_combine, (retain, driven), axis=0)[1]  46 us
    ppermute x2, starting transfers between devices, layer(): lax.ppermute(given, 'c', ring(c_count, 1))  23.6 us
    ppermute x6, starting transfers between devices, y_pieces(): pieces.append(lax.ppermute(rows, 'y', ring(count, step)))  20 us
    ppermute x6, waiting for transfers between devices, y_pieces(): pieces.append(lax.ppermute(rows, 'y', ring(count, step)))  15.8 us
    all_to_all x1, blocking collectives, x_summed(): arrived = lax.all_to_all(tiles, 'x', 0, 0, tiled=True)  15.5 us
    all_gather x1, blocking collectives, layer(): mine = lax.all_gather(normed_mid, 'x', axis=0, tiled=True)  11.7 us
    dynamic_update_slice x8, local copies, waits for them, and re-layouts, placed(): whole = lax.dynamic_update_slice_in_dim(whole, tiles, origin, 1)  11.6 us
  transfers between devices with their start and end apart: 10, of which 5 were waited for; matrix products, arithmetic and copies ran while one was open for 6% of the time, Pallas kernels for 0%

profile of v1, /device:TPU:1, one launch (start us, length us, event | category | flops | bytes accessed | tf_op | source)
XLA Modules:
  0.0 266.4 jit_solution(10907422739044820783)
XLA Ops:
  3.5 63.7 %all-gather.1 = f16[512,1408]{1,0:T(8,128)(2,1)S(1)} all-gather(f16[16,1408]{1,0:T(8,128)(2,1)S(1)} %multiply_convert_fusion.1), channel_id=1, replica_groups=mesh['z'=32,'y'=4,'x'=4,'c'=2] {'z'}, dimensions={0}, use_global_device_ids=true | all-gather | bytes 1486848 | tf_op jit(solution)/shard_map/all_gather | solution.py:113
  67.6 3.3 %collective-permute-start = (bf16[512,384]{1,0:T(8,128)(2,1)S(1)}, bf16[512,384]{1,0:T(8,128)(2,1)}, u32[]{:S(2)}, u32[]{:S(2)}) collective-permute-start(bf16[512,384]{1,0:T(8,128)(2,1)S(1)} %slice.287), channel_id=1, source_target_pairs={{0,8},{8,16},{16,24},{24,0},{1,9},{9,17},{17,25},{25,1},{2,10},{10... | collective-permute-start | bytes 1179656 | tf_op jit(solution)/shard_map/ppermute | solution.py:54
  70.9 3.4 %collective-permute-start.1 = (bf16[512,384]{1,0:T(8,128)(2,1)S(1)}, bf16[512,384]{1,0:T(8,128)(2,1)}, u32[]{:S(2)}, u32[]{:S(2)}) collective-permute-start(bf16[512,384]{1,0:T(8,128)(2,1)S(1)} %slice.287), channel_id=1, source_target_pairs={{0,24},{8,0},{16,8},{24,16},{1,25},{9,1},{17,9},{25,17},{2,26},{10... | collective-permute-start | bytes 1179656 | tf_op jit(solution)/shard_map/ppermute | solution.py:54
  74.3 3.5 %collective-permute-start.2 = (bf16[512,384]{1,0:T(8,128)(2,1)S(1)}, bf16[512,384]{1,0:T(8,128)(2,1)}, u32[]{:S(2)}, u32[]{:S(2)}) collective-permute-start(bf16[512,384]{1,0:T(8,128)(2,1)S(1)} %slice.287), channel_id=1, source_target_pairs={{0,16},{8,24},{16,0},{24,8},{1,17},{9,25},{17,1},{25,9},{2,18},{10... | collective-permute-start | bytes 1179656 | tf_op jit(solution)/shard_map/ppermute | solution.py:54
  81.0 3.5 %collective-permute-done.2 = bf16[512,384]{1,0:T(8,128)(2,1)} collective-permute-done((bf16[512,384]{1,0:T(8,128)(2,1)S(1)}, bf16[512,384]{1,0:T(8,128)(2,1)}, u32[]{:S(2)}, u32[]{:S(2)}) %collective-permute-start.2) | collective-permute-done | bytes 393248 | tf_op jit(solution)/shard_map/ppermute | solution.py:54
  89.2 1.7 fusion.80
  96.6 1.5 fusion.90
  98.0 1.4 slice.238
  99.5 1.4 slice.243
  100.9 1.4 slice.239
  102.3 1.4 slice.281
  103.7 1.4 slice.241
  105.1 1.4 slice.240
  106.5 1.4 fusion.91
  107.9 1.3 slice.249
  109.2 1.3 slice.245
  110.6 1.3 slice.247
  111.9 1.3 slice.246
  113.2 1.4 fusion.92
  114.6 1.3 slice.250
  115.9 1.3 slice.255
  117.2 1.3 slice.251
  120.3 1.3 fusion.93
  122.9 1.3 slice.257
  124.2 1.3 slice.259
  125.5 1.3 slice.258
  126.8 1.3 fusion.94
  138.7 1.3 slice.244
  154.2 2.1 fusion.71
  156.7 17.9 %collective-permute-start.3 = (bf16[192,2048]{1,0:T(8,128)(2,1)S(1)}, bf16[192,2048]{1,0:T(8,128)(2,1)S(1)}, u32[]{:S(2)}, u32[]{:S(2)}) collective-permute-start(bf16[192,2048]{1,0:T(8,128)(2,1)S(1)} %convolution_convert_fusion.2), channel_id=1, source_target_pairs={{0,1},{1,0},{2,3},{3,2},{4,5},{5,4},{6,7},{7,6},{8,9},{9,8},{10,11... | collective-permute-start | bytes 2359304 | tf_op jit(solution)/shard_map/ppermute | solution.py:143
  174.6 1.9 collective-permute-done.3
  177.8 4.0 %all-to-all-start = ((bf16[4,48,2048]{2,1,0:T(8,128)(2,1)}), bf16[4,48,2048]{2,1,0:T(8,128)(2,1)S(1)}, u32[]{:S(2)}, u32[]{:S(2)}) async-start(bf16[4,48,2048]{2,1,0:T(8,128)(2,1)} %bitcast.47), calls=%async_computation | async-start | bytes 1572864 | tf_op jit(solution)/shard_map/all_to_all | solution.py:73
  181.9 3.1 %collective-permute-start.4 = (bf16[512,1024]{1,0:T(8,128)(2,1)S(1)}, bf16[512,1024]{1,0:T(8,128)(2,1)}, u32[]{:S(2)}, u32[]{:S(2)}) collective-permute-start(bf16[512,1024]{1,0:T(8,128)(2,1)S(1)} %slice.304), channel_id=1, source_target_pairs={{0,8},{8,16},{16,24},{24,0},{1,9},{9,17},{17,25},{25,1},{2,10},{10... | collective-permute-start | bytes 3145736 | tf_op jit(solution)/shard_map/ppermute | solution.py:54
  185.0 3.6 %collective-permute-start.5 = (bf16[512,1024]{1,0:T(8,128)(2,1)S(1)}, bf16[512,1024]{1,0:T(8,128)(2,1)}, u32[]{:S(2)}, u32[]{:S(2)}) collective-permute-start(bf16[512,1024]{1,0:T(8,128)(2,1)S(1)} %slice.304), channel_id=1, source_target_pairs={{0,24},{8,0},{16,8},{24,16},{1,25},{9,1},{17,9},{25,17},{2,26},{10... | collective-permute-start | bytes 3145736 | tf_op jit(solution)/shard_map/ppermute | solution.py:54
  188.6 3.1 %collective-permute-start.6 = (bf16[512,1024]{1,0:T(8,128)(2,1)S(1)}, bf16[512,1024]{1,0:T(8,128)(2,1)}, u32[]{:S(2)}, u32[]{:S(2)}) collective-permute-start(bf16[512,1024]{1,0:T(8,128)(2,1)S(1)} %slice.304), channel_id=1, source_target_pairs={{0,16},{8,24},{16,0},{24,8},{1,17},{9,25},{17,1},{25,9},{2,18},{10... | collective-permute-start | bytes 3145736 | tf_op jit(solution)/shard_map/ppermute | solution.py:54
  191.7 1.8 all-to-all-done
  194.9 11.7 %all_gather.7 = bf16[192,2048]{1,0:T(8,128)(2,1)S(1)} all-gather(bf16[48,2048]{1,0:T(8,128)(2,1)S(1)} %fusion.53), channel_id=1, replica_groups=mesh['z'=32,'y'=4,'x'=4,'c'=2] {'x'}, dimensions={0}, use_global_device_ids=true | all-gather | bytes 983040 | tf_op jit(solution)/shard_map/all_gather | solution.py:150
  206.6 5.8 %collective-permute-start.7 = (bf16[192,2048]{1,0:T(8,128)(2,1)S(1)}, bf16[192,2048]{1,0:T(8,128)(2,1)S(1)}, u32[]{:S(2)}, u32[]{:S(2)}) collective-permute-start(bf16[192,2048]{1,0:T(8,128)(2,1)S(1)} %all_gather.7), channel_id=1, source_target_pairs={{0,1},{1,0},{2,3},{3,2},{4,5},{5,4},{6,7},{7,6},{8,9},{9,8},{10,11... | collective-permute-start | bytes 2359304 | tf_op jit(solution)/shard_map/ppermute | solution.py:151
  212.4 2.5 broadcast_in_dim.5
  215.9 2.4 constant_dynamic-update-slice_fusion.7
  218.3 2.3 constant_dynamic-update-slice_fusion.6
  220.7 12.3 %collective-permute-done.6 = bf16[512,1024]{1,0:T(8,128)(2,1)} collective-permute-done((bf16[512,1024]{1,0:T(8,128)(2,1)S(1)}, bf16[512,1024]{1,0:T(8,128)(2,1)}, u32[]{:S(2)}, u32[]{:S(2)}) %collective-permute-start.6) | collective-permute-done | bytes 1048608 | tf_op jit(solution)/shard_map/ppermute | solution.py:54
  233.0 2.4 constant_dynamic-update-slice_fusion.5
  235.4 3.5 %convolution_convert_fusion = bf16[192,2048]{1,0:T(8,128)(2,1)S(1)} fusion(bf16[2048,1024]{1,0:T(8,128)(2,1)} %bitcast.22, bf16[192,2048]{1,0:T(8,128)(2,1)S(1)} %collective-permute-done.7), kind=kOutput, calls=%fused_computation.6 | convolution fusion | flops 805994496 | bytes 5767168 | tf_op jit(solution)/shard_map/dot_general | solution.py:45
  238.9 5.7 %collective-permute-start.8 = (bf16[192,2048]{1,0:T(8,128)(2,1)S(1)}, bf16[192,2048]{1,0:T(8,128)(2,1)S(1)}, u32[]{:S(2)}, u32[]{:S(2)}) collective-permute-start(bf16[192,2048]{1,0:T(8,128)(2,1)S(1)} %convolution_convert_fusion), channel_id=1, source_target_pairs={{0,1},{1,0},{2,3},{3,2},{4,5},{5,4},{6,7},{7,6},{8,9},{9,8},{10,11... | collective-permute-start | bytes 2359304 | tf_op jit(solution)/shard_map/ppermute | solution.py:160
  244.6 1.9 collective-permute-done.8
  246.5 3.5 %fusion.5 = bf16[192,2048]{1,0:T(8,128)(2,1)S(1)} fusion(bf16[2048,1024]{1,0:T(8,128)(2,1)} %bitcast.22, bf16[192,2048]{1,0:T(8,128)(2,1)S(1)} %collective-permute-done.8, bf16[192,2048]{1,0:T(8,128)(2,1)S(1)} %all_gather.7), kind=kOutput, calls=%fused_computation.10 | convolution fusion | flops 807567360 | bytes 6553600 | tf_op jit(solution)/shard_map/dot_general | solution.py:45
  250.0 15.5 %all_to_all.10 = bf16[4,48,2048]{2,1,0:T(8,128)(2,1)S(1)} all-to-all(bf16[4,48,2048]{2,1,0:T(8,128)(2,1)S(1)} %bitcast.49), channel_id=1, replica_groups=mesh['z'=32,'y'=4,'x'=4,'c'=2] {'x'}, dimensions={0} | all-to-all | bytes 1572864 | tf_op jit(solution)/shard_map/all_to_all | solution.py:73
  (138 shorter events, 49.9 us)
Async XLA Ops:
  0.0 87.1 %copy-start = (bf16[2,64,64]{2,1,0:T(8,128)(2,1)S(1)}, bf16[2,64,64]{2,1,0:T(8,128)(2,1)}, u32[]{:S(2)}) copy-start(bf16[2,64,64]{2,1,0:T(8,128)(2,1)} %param.18) | copy-start | bytes 49156
  67.3 10.6 %copy-start.1 = (bf16[384,2048]{1,0:T(8,128)(2,1)S(1)}, bf16[384,2048]{1,0:T(8,128)(2,1)}, u32[]{:S(2)}) copy-start(bf16[384,2048]{1,0:T(8,128)(2,1)} %param.13) | copy-start | bytes 4718596
  67.5 10.7 %copy-start.7 = (bf16[4,128]{1,0:T(4,128)(2,1)S(1)}, bf16[4,128]{1,0:T(4,128)(2,1)}, u32[]{:S(2)}) copy-start(bf16[4,128]{1,0:T(4,128)(2,1)} %param.17) | copy-start | bytes 3076
  67.5 10.8 %copy-start.12 = (f32[128]{0:T(128)S(1)}, f32[128]{0:T(128)}, u32[]{:S(2)}) copy-start(f32[128]{0:T(128)} %param.20) | copy-start | bytes 1540
  67.6 11.1 %collective-permute-start = (bf16[512,384]{1,0:T(8,128)(2,1)S(1)}, bf16[512,384]{1,0:T(8,128)(2,1)}, u32[]{:S(2)}, u32[]{:S(2)}) collective-permute-start(bf16[512,384]{1,0:T(8,128)(2,1)S(1)} %slice.287), channel_id=1, source_target_pairs={{0,8},{8,16},{16,24},{24,0},{1,9},{9,17},{17,25},{25,1},{2,10},{10... | collective-permute-start | bytes 1179656 | tf_op jit(solution)/shard_map/ppermute | solution.py:54
  70.9 9.0 %collective-permute-start.1 = (bf16[512,384]{1,0:T(8,128)(2,1)S(1)}, bf16[512,384]{1,0:T(8,128)(2,1)}, u32[]{:S(2)}, u32[]{:S(2)}) collective-permute-start(bf16[512,384]{1,0:T(8,128)(2,1)S(1)} %slice.287), channel_id=1, source_target_pairs={{0,24},{8,0},{16,8},{24,16},{1,25},{9,1},{17,9},{25,17},{2,26},{10... | collective-permute-start | bytes 1179656 | tf_op jit(solution)/shard_map/ppermute | solution.py:54
  74.3 10.1 %collective-permute-start.2 = (bf16[512,384]{1,0:T(8,128)(2,1)S(1)}, bf16[512,384]{1,0:T(8,128)(2,1)}, u32[]{:S(2)}, u32[]{:S(2)}) collective-permute-start(bf16[512,384]{1,0:T(8,128)(2,1)S(1)} %slice.287), channel_id=1, source_target_pairs={{0,16},{8,24},{16,0},{24,8},{1,17},{9,25},{17,1},{25,9},{2,18},{10... | collective-permute-start | bytes 1179656 | tf_op jit(solution)/shard_map/ppermute | solution.py:54
  78.3 7.2 %copy-start.8 = (f32[384]{0:T(512)}, f32[384]{0:T(512)S(1)}, u32[]{:S(2)}) copy-start(f32[384]{0:T(512)S(1)} %add_rsqrt_fusion) | copy-start | bytes 4612
  78.6 6.9 %copy-start.2 = (bf16[384,2048]{1,0:T(8,128)(2,1)S(1)}, bf16[384,2048]{1,0:T(8,128)(2,1)}, u32[]{:S(2)}) copy-start(bf16[384,2048]{1,0:T(8,128)(2,1)} %param.13) | copy-start | bytes 4718596
  78.6 6.9 %copy-start.11 = (f32[2048]{0:T(1024)S(1)}, f32[2048]{0:T(1024)}, u32[]{:S(2)}) copy-start(f32[2048]{0:T(1024)} %param.14) | copy-start | bytes 24580
  86.2 0.7 copy-start.3
  86.2 2.0 copy-start.10
  98.0 56.0 %copy-start.4 = (f32[191,128]{1,0:T(8,128)S(1)}, f32[191,128]{1,0:T(8,128)}, u32[]{:S(2)}) copy-start(f32[191,128]{1,0:T(8,128)} %slice.226) | copy-start | bytes 293380
  143.7 10.4 %copy-start.5 = (f32[191,128]{1,0:T(8,128)S(1)}, f32[191,128]{1,0:T(8,128)}, u32[]{:S(2)}) copy-start(f32[191,128]{1,0:T(8,128)} %slice.285) | copy-start | bytes 293380
  147.6 6.5 %copy-start.9 = (f32[1,128]{1,0:T(1,128)S(1)}, f32[1,128]{1,0:T(1,128)}, u32[]{:S(2)}) copy-start(f32[1,128]{1,0:T(1,128)} %slice.288) | copy-start | bytes 1540
  156.7 19.8 %collective-permute-start.3 = (bf16[192,2048]{1,0:T(8,128)(2,1)S(1)}, bf16[192,2048]{1,0:T(8,128)(2,1)S(1)}, u32[]{:S(2)}, u32[]{:S(2)}) collective-permute-start(bf16[192,2048]{1,0:T(8,128)(2,1)S(1)} %convolution_convert_fusion.2), channel_id=1, source_target_pairs={{0,1},{1,0},{2,3},{3,2},{4,5},{5,4},{6,7},{7,6},{8,9},{9,8},{10,11... | collective-permute-start | bytes 2359304 | tf_op jit(solution)/shard_map/ppermute | solution.py:143
  177.8 15.7 %all-to-all-start = ((bf16[4,48,2048]{2,1,0:T(8,128)(2,1)}), bf16[4,48,2048]{2,1,0:T(8,128)(2,1)S(1)}, u32[]{:S(2)}, u32[]{:S(2)}) async-start(bf16[4,48,2048]{2,1,0:T(8,128)(2,1)} %bitcast.47), calls=%async_computation | async-start | bytes 1572864 | tf_op jit(solution)/shard_map/all_to_all | solution.py:73
  181.8 13.0 %copy-start.6 = (f32[2048]{0:T(1024)S(1)}, f32[2048]{0:T(1024)}, u32[]{:S(2)}) copy-start(f32[2048]{0:T(1024)} %param.23) | copy-start | bytes 24580
  181.9 34.0 %collective-permute-start.4 = (bf16[512,1024]{1,0:T(8,128)(2,1)S(1)}, bf16[512,1024]{1,0:T(8,128)(2,1)}, u32[]{:S(2)}, u32[]{:S(2)}) collective-permute-start(bf16[512,1024]{1,0:T(8,128)(2,1)S(1)} %slice.304), channel_id=1, source_target_pairs={{0,8},{8,16},{16,24},{24,0},{1,9},{9,17},{17,25},{25,1},{2,10},{10... | collective-permute-start | bytes 3145736 | tf_op jit(solution)/shard_map/ppermute | solution.py:54
  185.0 33.4 %collective-permute-start.5 = (bf16[512,1024]{1,0:T(8,128)(2,1)S(1)}, bf16[512,1024]{1,0:T(8,128)(2,1)}, u32[]{:S(2)}, u32[]{:S(2)}) collective-permute-start(bf16[512,1024]{1,0:T(8,128)(2,1)S(1)} %slice.304), channel_id=1, source_target_pairs={{0,24},{8,0},{16,8},{24,16},{1,25},{9,1},{17,9},{25,17},{2,26},{10... | collective-permute-start | bytes 3145736 | tf_op jit(solution)/shard_map/ppermute | solution.py:54
  188.6 44.4 %collective-permute-start.6 = (bf16[512,1024]{1,0:T(8,128)(2,1)S(1)}, bf16[512,1024]{1,0:T(8,128)(2,1)}, u32[]{:S(2)}, u32[]{:S(2)}) collective-permute-start(bf16[512,1024]{1,0:T(8,128)(2,1)S(1)} %slice.304), channel_id=1, source_target_pairs={{0,16},{8,24},{16,0},{24,8},{1,17},{9,25},{17,1},{25,9},{2,18},{10... | collective-permute-start | bytes 3145736 | tf_op jit(solution)/shard_map/ppermute | solution.py:54
  206.6 28.8 %collective-permute-start.7 = (bf16[192,2048]{1,0:T(8,128)(2,1)S(1)}, bf16[192,2048]{1,0:T(8,128)(2,1)S(1)}, u32[]{:S(2)}, u32[]{:S(2)}) collective-permute-start(bf16[192,2048]{1,0:T(8,128)(2,1)S(1)} %all_gather.7), channel_id=1, source_target_pairs={{0,1},{1,0},{2,3},{3,2},{4,5},{5,4},{6,7},{7,6},{8,9},{9,8},{10,11... | collective-permute-start | bytes 2359304 | tf_op jit(solution)/shard_map/ppermute | solution.py:151
  238.9 7.6 %collective-permute-start.8 = (bf16[192,2048]{1,0:T(8,128)(2,1)S(1)}, bf16[192,2048]{1,0:T(8,128)(2,1)S(1)}, u32[]{:S(2)}, u32[]{:S(2)}) collective-permute-start(bf16[192,2048]{1,0:T(8,128)(2,1)S(1)} %convolution_convert_fusion), channel_id=1, source_target_pairs={{0,1},{1,0},{2,3},{3,2},{4,5},{5,4},{6,7},{7,6},{8,9},{9,8},{10,11... | collective-permute-start | bytes 2359304 | tf_op jit(solution)/shard_map/ppermute | solution.py:160

commit v2 on v1

v2 whole, which is shorter than its diff:
```python
import jax
import jax.numpy as jnp
from jax import lax
from jax.experimental import pallas as pl
from jax.experimental.pallas import tpu as pltpu
from jax.sharding import Mesh, PartitionSpec as P


epsilon = 1e-06
decay_rate_scale = 8.0
wire_scale = 65536.0
row_scale = 512.0


def ring(count, step):
    return [(k, (k + step) % count) for k in range(count)]


def rms_scaled(rows, scales):
    widened = rows.astype(jnp.float32)
    mean_square = jnp.mean(widened * widened, axis=-1, keepdims=True)
    return (widened * lax.rsqrt(mean_square + epsilon) * scales).astype(jnp.bfloat16)


def shifted(rows, step, fill):
    index = lax.broadcasted_iota(jnp.int32, rows.shape, 0)
    return jnp.where(index >= step, pltpu.roll(rows, step, 0), fill)


def one_minus_exp(value):
    terms = 1.0 + value * (1.0 / 8.0)
    for order in (7.0, 6.0, 5.0, 4.0, 3.0, 2.0):
        terms = 1.0 + value * (1.0 / order) * terms
    return jnp.where(value > -0.3, -value * terms, 1.0 - jnp.exp(value))


def assemble(pieces, whole):
    me = lax.axis_index("y")
    for step, piece in zip((0, 1, 3, 2), pieces):
        whole[:, lax.rem(me + 4 - step, 4)] = piece[...]


def join_kernel(a_ref, b_ref, c_ref, d_ref, e_ref, out_ref):
    begin = 0
    for ref in (a_ref, b_ref, c_ref, d_ref, e_ref):
        stop = begin + ref.shape[1]
        out_ref[:, begin:stop] = ref[...] * jnp.asarray(wire_scale, ref.dtype)
        begin = stop


def mixer_kernel(
    normed, taps, gates, decay, extra, p0, p1, p2, p3, given, kept, whole, kept_rows
):
    positions, channels = extra.shape
    core = lax.axis_index("c")
    assemble((p0, p1, p2, p3), whole)
    weights = whole[...].reshape(normed.shape[1], 3 * channels)
    both = jnp.dot(
        normed[...], weights[:, : 2 * channels], preferred_element_type=jnp.float32
    )
    branch = both[:, :channels].astype(jnp.bfloat16).astype(jnp.float32)
    gate = both[:, channels:].astype(jnp.bfloat16).astype(jnp.float32)
    tap = taps[...].astype(jnp.float32)
    running = branch * tap[3:4]
    for back in (1, 2, 3):
        running = running + shifted(branch, back, 0.0) * tap[3 - back : 4 - back]
    convolved = running.astype(jnp.bfloat16)
    mapped = jax.nn.sigmoid(
        jnp.dot(convolved, gates[...], preferred_element_type=jnp.float32)
    )
    log_keep = mapped[:, :channels] * decay[...] + extra[...]
    retain = jnp.exp(log_keep)
    memory = jnp.sqrt(one_minus_exp(2.0 * log_keep)) * (
        mapped[:, channels:] * convolved.astype(jnp.float32)
    )
    step = 1
    while step < positions:
        memory = retain * shifted(memory, step, 0.0) + memory
        retain = retain * shifted(retain, step, 1.0)
        step *= 2
    inner = 0.7978845608028654 * (gate + 0.044715 * gate * gate * gate)
    recurrent = (memory * (0.5 * gate * (1.0 + jnp.tanh(inner)))).astype(jnp.bfloat16)
    kept_rows[...] = recurrent.reshape(kept_rows.shape)
    out_rows = weights[:, 2 * channels :]
    for ref, which in ((given, 1 - core), (kept, core)):
        rows = kept_rows[:, which].reshape(positions // 2, channels)
        ref[...] = contract_columns(rows, out_rows).astype(jnp.bfloat16)


def channel_kernel(rows, p0, p1, p2, p3, given, kept, whole, hidden_rows):
    positions, width = rows.shape
    core = lax.axis_index("c")
    assemble((p0, p1, p2, p3), whole)
    half = whole.shape[3] // 2
    weights = whole[...].reshape(width, 2 * half)
    raised = jnp.dot(rows[...], weights[:, :half], preferred_element_type=jnp.float32)
    hidden = jnp.square(jnp.maximum(raised, 0.0)).astype(jnp.bfloat16)
    hidden_rows[...] = hidden.reshape(hidden_rows.shape)
    for ref, which in ((given, 1 - core), (kept, core)):
        picked = hidden_rows[:, which].reshape(positions // 2, half)
        ref[...] = contract_columns(picked, weights[:, half:]).astype(jnp.bfloat16)


def contract_columns(left, right):
    return lax.dot_general(
        left, right, (((1,), (1,)), ((), ())), preferred_element_type=jnp.float32
    )


def in_vmem(count):
    return [pl.BlockSpec(memory_space=pltpu.VMEM)] * count


def mixed(kernel, operands, pieces, scratch_rows, flops):
    z_count, height, columns = pieces[0].shape
    half = jax.ShapeDtypeStruct((operands[0].shape[0] // 2, operands[0].shape[1]), jnp.bfloat16)
    return pl.pallas_call(
        kernel,
        out_shape=(half, half),
        in_specs=in_vmem(len(operands) + len(pieces)),
        out_specs=tuple(in_vmem(2)),
        scratch_shapes=[
            pltpu.VMEM((z_count, len(pieces), height, columns), jnp.bfloat16),
            pltpu.VMEM(scratch_rows, jnp.bfloat16),
        ],
        compiler_params=pltpu.CompilerParams(vmem_limit_bytes=24 << 20),
        cost_estimate=pl.CostEstimate(flops=flops, bytes_accessed=8 << 20, transcendentals=0),
    )(*operands, *pieces)


def y_pieces(rows, height):
    count = lax.axis_size("y")
    pieces = [rows]
    for step in (1, count - 1, 2):
        pieces.append(lax.ppermute(rows, "y", ring(count, step)))
    return [piece.reshape(-1, height, rows.shape[1]) for piece in pieces]


def x_summed(rows):
    count = lax.axis_size("x")
    tiles = rows.reshape(count, rows.shape[0] // count, rows.shape[1])
    arrived = lax.all_to_all(tiles, "x", 0, 0, tiled=True)
    return arrived.astype(jnp.float32).sum(axis=0)


def added(left, right):
    return (left.astype(jnp.float32) + right.astype(jnp.float32)).astype(jnp.bfloat16)


def layer(
    tokens,
    first_norm_scale,
    recurrent_branch_matrix,
    gelu_gate_matrix,
    filter_taps_weight,
    recurrence_gate_blocks,
    input_gate_blocks,
    base_decay_logits,
    extra_log_decay,
    mixer_output_matrix,
    second_norm_scale,
    mixer_up_matrix,
    mixer_down_matrix,
):
    positions, width = tokens.shape
    _, x_count, c_count = (lax.axis_size(k) for k in ("z", "x", "c"))
    own_count = positions // (x_count * c_count)
    x_index, c_index = lax.axis_index("x"), lax.axis_index("c")
    channels = recurrent_branch_matrix.shape[1]

    height = recurrent_branch_matrix.shape[0]
    matrices = (
        recurrent_branch_matrix,
        gelu_gate_matrix,
        mixer_output_matrix,
        mixer_up_matrix,
        mixer_down_matrix,
    )
    joined = pl.pallas_call(
        join_kernel,
        out_shape=jax.ShapeDtypeStruct((height, sum(k.shape[1] for k in matrices)), jnp.bfloat16),
        in_specs=in_vmem(len(matrices)),
        out_specs=in_vmem(1)[0],
        name="join",
    )(*matrices)
    z_rows = lax.all_gather(joined.astype(jnp.float16), "z", axis=0, tiled=True)
    z_rows = (z_rows.astype(jnp.float32) * (1.0 / wire_scale)).astype(jnp.bfloat16)
    first = y_pieces(z_rows[:, : 3 * channels], height)
    second = y_pieces(z_rows[:, 3 * channels :], height)

    normed = rms_scaled(tokens, first_norm_scale)
    diagonal = jnp.zeros((2, channels // 2, 2, 2, channels // 2), jnp.bfloat16)
    for group in range(2):
        diagonal = diagonal.at[group, :, 0, group].set(recurrence_gate_blocks[group])
        diagonal = diagonal.at[group, :, 1, group].set(input_gate_blocks[group])
    decay = (decay_rate_scale * jax.nn.log_sigmoid(base_decay_logits))[None]

    def given_summed(given, kept):
        return x_summed(added(kept, lax.ppermute(given, "c", ring(c_count, 1))))

    by_core = (x_count, c_count, own_count)
    given, kept = mixed(
        mixer_kernel,
        (normed, filter_taps_weight, diagonal.reshape(channels, -1), decay, extra_log_decay),
        first,
        (*by_core, channels),
        6 * positions * width * channels,
    )
    mixer_out = given_summed(given, kept)
    own_rows = lax.dynamic_slice_in_dim(
        tokens, (x_index * c_count + c_index) * own_count, own_count, 0
    )
    residual = (own_rows.astype(jnp.float32) + mixer_out).astype(jnp.bfloat16)
    normed_mid = rms_scaled(residual, second_norm_scale)
    sent = (normed_mid.astype(jnp.float32) * row_scale).astype(jnp.float16)
    arrived = lax.all_gather(sent, ("x", "c"), axis=0, tiled=True)
    rows = (arrived.astype(jnp.float32) * (1.0 / row_scale)).astype(jnp.bfloat16)
    given, kept = mixed(
        channel_kernel,
        (rows,),
        second,
        (*by_core, mixer_up_matrix.shape[1]),
        4 * positions * width * mixer_up_matrix.shape[1],
    )
    channel_sum = given_summed(given, kept)
    return (residual.astype(jnp.float32) + channel_sum).astype(jnp.bfloat16)


def solution(mesh):
    z_count = 32 if mesh.shape["fs"] == 128 else mesh.shape["fs"] // 4
    split = Mesh(
        mesh.devices.reshape(z_count, mesh.shape["fs"] // z_count, mesh.shape["tp"] // 2, 2),
        ("z", "y", "x", "c"),
    )
    fs, tp = ("z", "y"), ("x", "c")
    in_specs = (
        P(fs, None),
        P(),
        P(fs, tp),
        P(fs, tp),
        P(None, tp),
        P(tp, None, None),
        P(tp, None, None),
        P(tp),
        P(fs, tp),
        P(fs, tp),
        P(),
        P(fs, tp),
        P(fs, tp),
    )
    return jax.shard_map(
        layer, mesh=split, in_specs=in_specs, out_specs=P((*fs, *tp), None), check_vma=False
    )
```

time: 270 us -> 189 us (0.70)
  local copies, waits for them, and re-layouts: 66.6 us -> 0.56 us
  other arithmetic: 21.7 us -> 7.03 us
  matrix products: 11.9 us -> 0 us
  waiting for transfers between devices: 21.4 us -> 31.3 us
  starting transfers between devices: 53.4 us -> 45.3 us
  Pallas kernels: 0 us -> 8.03 us
  blocking collectives: 90.9 us -> 95.1 us
    slice x51 -> x2, local copies, waits for them, and re-layouts: 46.1 us -> 0.17 us  [the longest x1 0.13 us: layer(): second = y_pieces(z_rows[:, 3 * channels:], height)]
    dot_general x8 -> x0, matrix products: 11.9 us -> none  [the longest x4 8.69 us: contract_columns(): lax.dot_general(left, right, (((1,), (1,)), ((), ())), preferred_element_...]
    dynamic_update_slice x8 -> x0, local copies, waits for them, and re-layouts: 11.6 us -> none  [placed(): whole = lax.dynamic_update_slice_in_dim(whole, tiles, origin, 1)]
    ppermute x6, waiting for transfers between devices: 15.8 us -> 24.7 us  [y_pieces(): pieces.append(lax.ppermute(rows, 'y', ring(count, step)))]
    mul x9 -> x0, other arithmetic: 8.6 us -> none  [the longest x7 8.58 us: linear_combine(): return (earlier[0] * later[0], later[0] * earlier[1] + later[1])]
    pallas_call x0 -> x3, Pallas kernels: none -> 8.03 us  [the longest x2 6.62 us: mixed(): pl.pallas_call(kernel, out_shape=(half, half), in_specs=in_vmem(len(opera...]
    ppermute x3 -> x2, starting transfers between devices: 29.4 us -> 22 us  [given_summed(): return x_summed(added(kept, lax.ppermute(given, 'c', ring(c_count, 1))))]
    add x15 -> x0, other arithmetic: 4.48 us -> none  [the longest x8 4.42 us: linear_combine(): return (earlier[0] * later[0], later[0] * earlier[1] + later[1])]
  transfers between devices with their start and end apart: 10 -> 9, of which waited for: 5 -> 6; matrix products, arithmetic and copies ran while one was open for 6% -> 2% of each run, Pallas kernels for 0% -> 0%
where the time goes in v2:
time: 189 us; the launch traced here: 188 us
  blocking collectives  95.1 us (50%)
  starting transfers between devices  45.3 us (24%)
  waiting for transfers between devices  31.3 us (17%)
  Pallas kernels  8.03 us (4%)
  other arithmetic  7.03 us (4%)
    all_gather x1, blocking collectives, layer(): z_rows = lax.all_gather(joined.astype(jnp.float16), 'z', axis=0, tiled=True)  63.7 us
    ppermute x6, waiting for transfers between devices, y_pieces(): pieces.append(lax.ppermute(rows, 'y', ring(count, step)))  24.7 us
    ppermute x2, starting transfers between devices, given_summed(): return x_summed(added(kept, lax.ppermute(given, 'c', ring(c_count, 1))))  22 us
    ppermute x6, starting transfers between devices, y_pieces(): pieces.append(lax.ppermute(rows, 'y', ring(count, step)))  19.1 us
    all_gather x1, blocking collectives, layer(): arrived = lax.all_gather(sent, ('x', 'c'), axis=0, tiled=True)  15.9 us
    all_to_all x1, blocking collectives, x_summed(): arrived = lax.all_to_all(tiles, 'x', 0, 0, tiled=True)  15.4 us
    pallas_call x2, Pallas kernels, mixed(): pl.pallas_call(kernel, out_shape=(half, half), in_specs=in_vmem(len(opera...  6.62 us
    all_to_all x1, starting transfers between devices, x_summed(): arrived = lax.all_to_all(tiles, 'x', 0, 0, tiled=True)  4.19 us
  transfers between devices with their start and end apart: 9, of which 6 were waited for; matrix products, arithmetic and copies ran while one was open for 2% of the time, Pallas kernels for 0%

profile of v2, /device:TPU:1, one launch (start us, length us, event | category | flops | bytes accessed | tf_op | source)
XLA Modules:
  0.0 187.7 jit_solution(3416642626502617540)
XLA Ops:
  0.0 1.4 join.1
  1.4 0.8 convert_element_type.70
  2.2 63.7 %all-gather.2 = f16[512,1408]{1,0:T(8,128)(2,1)S(1)} all-gather(f16[16,1408]{1,0:T(8,128)(2,1)S(1)} %convert_element_type.70), channel_id=1, replica_groups=mesh['z'=32,'y'=4,'x'=4,'c'=2] {'z'}, dimensions={0}, use_global_device_ids=true | all-gather | bytes 1486848 | tf_op jit(solution)/shard_map/all_gather | solution.py:186
  65.9 0.3 multiply_convert_fusion.1
  66.2 0.0 copy-start.5
  66.2 0.0 copy-start.6
  66.2 0.0 copy-start.9
  66.2 0.0 copy-start.7
  66.3 3.3 %collective-permute-start = (bf16[512,384]{1,0:T(8,128)(2,1)S(1)}, bf16[512,384]{1,0:T(8,128)(2,1)S(1)}, u32[]{:S(2)}, u32[]{:S(2)}) collective-permute-start(bf16[512,384]{1,0:T(8,128)(2,1)S(1)} %slice.163), channel_id=1, source_target_pairs={{0,8},{8,16},{16,24},{24,0},{1,9},{9,17},{17,25},{25,1},{2,10},{10... | collective-permute-start | bytes 1179656 | tf_op jit(solution)/shard_map/ppermute | solution.py:135
  69.6 3.4 %collective-permute-start.1 = (bf16[512,384]{1,0:T(8,128)(2,1)S(1)}, bf16[512,384]{1,0:T(8,128)(2,1)S(1)}, u32[]{:S(2)}, u32[]{:S(2)}) collective-permute-start(bf16[512,384]{1,0:T(8,128)(2,1)S(1)} %slice.163), channel_id=1, source_target_pairs={{0,24},{8,0},{16,8},{24,16},{1,25},{9,1},{17,9},{25,17},{2,26},{10... | collective-permute-start | bytes 1179656 | tf_op jit(solution)/shard_map/ppermute | solution.py:135
  73.0 3.5 %collective-permute-start.2 = (bf16[512,384]{1,0:T(8,128)(2,1)S(1)}, bf16[512,384]{1,0:T(8,128)(2,1)S(1)}, u32[]{:S(2)}, u32[]{:S(2)}) collective-permute-start(bf16[512,384]{1,0:T(8,128)(2,1)S(1)} %slice.163), channel_id=1, source_target_pairs={{0,16},{8,24},{16,0},{24,8},{1,17},{9,25},{17,1},{25,9},{2,18},{10... | collective-permute-start | bytes 1179656 | tf_op jit(solution)/shard_map/ppermute | solution.py:135
  76.6 0.4 fusion
  77.1 0.1 copy.14
  77.2 0.1 reshape.225.gates
  77.4 0.0 copy-done.9
  77.4 0.0 copy-start
  77.4 0.0 copy-start.1
  77.4 0.4 fusion.2.normed
  77.9 0.0 collective-permute-done
  77.9 0.3 collective-permute-done.1
  78.2 4.9 %collective-permute-done.2 = bf16[512,384]{1,0:T(8,128)(2,1)S(1)} collective-permute-done((bf16[512,384]{1,0:T(8,128)(2,1)S(1)}, bf16[512,384]{1,0:T(8,128)(2,1)S(1)}, u32[]{:S(2)}, u32[]{:S(2)}) %collective-permute-start.2) | collective-permute-done | bytes 393248 | tf_op jit(solution)/shard_map/ppermute | solution.py:135
  83.0 0.0 copy-done
  83.0 2.7 %shard_map.127 = (bf16[192,2048]{1,0:T(8,128)(2,1)S(1)}, bf16[192,2048]{1,0:T(8,128)(2,1)S(1)}) custom-call(bf16[384,2048]{1,0:T(8,128)(2,1)S(1)} %fusion.2.normed, bf16[4,128]{1,0:T(4,128)(2,1)S(1)} %copy-done.1, bf16[128,256]{1,0:T(8,128)(2,1)S(1)} %reshape.225.gates, f32[1,128]{1,0:T(1,128)S(1)} %multiply_bitcast_fusion.decay, f32[384,128]{1,0:T(8,128)S(1)} %copy-done, ...), custom_call_target="tpu_custom_call" | custom-call | flops 603979776 | bytes 8388608 | tf_op jit(solution)/shard_map/pallas_call | solution.py:117
  85.8 17.9 %collective-permute-start.3 = (bf16[192,2048]{1,0:T(8,128)(2,1)S(1)}, bf16[192,2048]{1,0:T(8,128)(2,1)S(1)}, u32[]{:S(2)}, u32[]{:S(2)}) collective-permute-start(bf16[192,2048]{1,0:T(8,128)(2,1)S(1)} %get-tuple-element.58), channel_id=1, source_target_pairs={{0,1},{1,0},{2,3},{3,2},{4,5},{5,4},{6,7},{7,6},{8,9},{9,8},{10,11... | collective-permute-start | bytes 2359304 | tf_op jit(solution)/shard_map/ppermute | solution.py:199
  103.7 1.9 %collective-permute-done.3 = bf16[192,2048]{1,0:T(8,128)(2,1)S(1)} collective-permute-done((bf16[192,2048]{1,0:T(8,128)(2,1)S(1)}, bf16[192,2048]{1,0:T(8,128)(2,1)S(1)}, u32[]{:S(2)}, u32[]{:S(2)}) %collective-permute-start.3) | collective-permute-done | bytes 786464 | tf_op jit(solution)/shard_map/ppermute | solution.py:199
  105.6 1.2 add_convert_fusion.1
  106.8 4.2 %all-to-all-start = ((bf16[4,48,2048]{2,1,0:T(8,128)(2,1)}), bf16[4,48,2048]{2,1,0:T(8,128)(2,1)}, u32[]{:S(2)}, u32[]{:S(2)}) async-start(bf16[4,48,2048]{2,1,0:T(8,128)(2,1)} %bitcast.9), calls=%async_computation | async-start | bytes 1572864 | tf_op jit(solution)/shard_map/all_to_all | solution.py:142
  111.0 0.0 copy-start.8
  111.0 0.1 slice.164
  111.1 3.1 %collective-permute-start.4 = (bf16[512,1024]{1,0:T(8,128)(2,1)S(1)}, bf16[512,1024]{1,0:T(8,128)(2,1)S(1)}, u32[]{:S(2)}, u32[]{:S(2)}) collective-permute-start(bf16[512,1024]{1,0:T(8,128)(2,1)S(1)} %slice.164), channel_id=1, source_target_pairs={{0,8},{8,16},{16,24},{24,0},{1,9},{9,17},{17,25},{25,1},{2,10},{10... | collective-permute-start | bytes 3145736 | tf_op jit(solution)/shard_map/ppermute | solution.py:135
  114.2 3.4 %collective-permute-start.5 = (bf16[512,1024]{1,0:T(8,128)(2,1)S(1)}, bf16[512,1024]{1,0:T(8,128)(2,1)S(1)}, u32[]{:S(2)}, u32[]{:S(2)}) collective-permute-start(bf16[512,1024]{1,0:T(8,128)(2,1)S(1)} %slice.164), channel_id=1, source_target_pairs={{0,24},{8,0},{16,8},{24,16},{1,25},{9,1},{17,9},{25,17},{2,26},{10... | collective-permute-start | bytes 3145736 | tf_op jit(solution)/shard_map/ppermute | solution.py:135
  117.6 2.4 %collective-permute-start.6 = (bf16[512,1024]{1,0:T(8,128)(2,1)S(1)}, bf16[512,1024]{1,0:T(8,128)(2,1)}, u32[]{:S(2)}, u32[]{:S(2)}) collective-permute-start(bf16[512,1024]{1,0:T(8,128)(2,1)S(1)} %slice.164), channel_id=1, source_target_pairs={{0,16},{8,24},{16,0},{24,8},{1,17},{9,25},{17,1},{25,9},{2,18},{10... | collective-permute-start | bytes 3145736 | tf_op jit(solution)/shard_map/ppermute | solution.py:135
  120.0 2.8 %all-to-all-done = bf16[4,48,2048]{2,1,0:T(8,128)(2,1)} async-done(((bf16[4,48,2048]{2,1,0:T(8,128)(2,1)}), bf16[4,48,2048]{2,1,0:T(8,128)(2,1)}, u32[]{:S(2)}, u32[]{:S(2)}) %all-to-all-start) | async-done | bytes 786464 | tf_op jit(solution)/shard_map/all_to_all | solution.py:142
  122.9 1.3 convert_reduce_fusion.1
  124.2 1.1 fusion.3
  125.3 0.1 multiply_convert_fusion.2
  125.5 15.9 %all-gather.3 = f16[384,2048]{1,0:T(8,128)(2,1)S(1)} all-gather(f16[48,2048]{1,0:T(8,128)(2,1)S(1)} %multiply_convert_fusion.2), channel_id=1, replica_groups=mesh['z'=32,'y'=4,'x'=4,'c'=2] {'x','c'}, dimensions={0}, use_global_device_ids=true | all-gather | bytes 1769472 | tf_op jit(solution)/shard_map/all_gather | solution.py:216
  141.4 0.3 multiply_convert_fusion.rows
  141.7 0.0 collective-permute-done.4
  141.7 0.0 collective-permute-done.5
  141.8 19.5 %collective-permute-done.6 = bf16[512,1024]{1,0:T(8,128)(2,1)} collective-permute-done((bf16[512,1024]{1,0:T(8,128)(2,1)S(1)}, bf16[512,1024]{1,0:T(8,128)(2,1)}, u32[]{:S(2)}, u32[]{:S(2)}) %collective-permute-start.6) | collective-permute-done | bytes 1048608 | tf_op jit(solution)/shard_map/ppermute | solution.py:135
  161.3 3.9 %shard_map.128 = (bf16[192,2048]{1,0:T(8,128)(2,1)S(1)}, bf16[192,2048]{1,0:T(8,128)(2,1)S(1)}) custom-call(bf16[384,2048]{1,0:T(8,128)(2,1)S(1)} %multiply_convert_fusion.rows, bf16[32,16,1024]{2,1,0:T(8,128)(2,1)S(1)} %bitcast.21, bf16[32,16,1024]{2,1,0:T(8,128)(2,1)S(1)} %bitcast.25, bf16[32,16,1024]{2,1,0:T(8,128)(2,1)S(1)} %bitcast.26, ...), custom_call_target="tpu_custom_call" | custom-call | flops 1610612736 | bytes 8388608 | tf_op jit(solution)/shard_map/pallas_call | solution.py:117
  165.2 4.1 %collective-permute-start.7 = (bf16[192,2048]{1,0:T(8,128)(2,1)S(1)}, bf16[192,2048]{1,0:T(8,128)(2,1)S(1)}, u32[]{:S(2)}, u32[]{:S(2)}) collective-permute-start(bf16[192,2048]{1,0:T(8,128)(2,1)S(1)} %get-tuple-element.60), channel_id=1, source_target_pairs={{0,1},{1,0},{2,3},{3,2},{4,5},{5,4},{6,7},{7,6},{8,9},{9,8},{10,11... | collective-permute-start | bytes 2359304 | tf_op jit(solution)/shard_map/ppermute | solution.py:199
  169.3 1.9 %collective-permute-done.7 = bf16[192,2048]{1,0:T(8,128)(2,1)S(1)} collective-permute-done((bf16[192,2048]{1,0:T(8,128)(2,1)S(1)}, bf16[192,2048]{1,0:T(8,128)(2,1)S(1)}, u32[]{:S(2)}, u32[]{:S(2)}) %collective-permute-start.7) | collective-permute-done | bytes 786464 | tf_op jit(solution)/shard_map/ppermute | solution.py:199
  171.2 0.3 add_convert_fusion
  171.4 15.4 %all_to_all.10 = bf16[4,48,2048]{2,1,0:T(8,128)(2,1)S(1)} all-to-all(bf16[4,48,2048]{2,1,0:T(8,128)(2,1)S(1)} %bitcast.27), channel_id=1, replica_groups=mesh['z'=32,'y'=4,'x'=4,'c'=2] {'x'}, dimensions={0} | all-to-all | bytes 1572864 | tf_op jit(solution)/shard_map/all_to_all | solution.py:142
  186.8 0.1 convert_reduce_fusion
  187.0 0.7 fusion.6
  (20 shorter events, 0.1 us)
Async XLA Ops:
  65.9 10.6 %copy-start.2 = (bf16[384,2048]{1,0:T(8,128)(2,1)S(1)}, bf16[384,2048]{1,0:T(8,128)(2,1)}, u32[]{:S(2)}) copy-start(bf16[384,2048]{1,0:T(8,128)(2,1)} %param.21) | copy-start | bytes 4718596
  66.2 10.9 %copy-start.3 = (bf16[512,1408]{1,0:T(8,128)(2,1)}, bf16[512,1408]{1,0:T(8,128)(2,1)S(1)}, u32[]{:S(2)}) copy-start(bf16[512,1408]{1,0:T(8,128)(2,1)S(1)} %multiply_convert_fusion.1) | copy-start | bytes 4325380
  66.2 10.8 %copy-start.5 = (bf16[2,64,64]{2,1,0:T(8,128)(2,1)S(1)}, bf16[2,64,64]{2,1,0:T(8,128)(2,1)}, u32[]{:S(2)}) copy-start(bf16[2,64,64]{2,1,0:T(8,128)(2,1)} %param.26) | copy-start | bytes 49156
  66.2 10.8 %copy-start.6 = (bf16[2,64,64]{2,1,0:T(8,128)(2,1)S(1)}, bf16[2,64,64]{2,1,0:T(8,128)(2,1)}, u32[]{:S(2)}) copy-start(bf16[2,64,64]{2,1,0:T(8,128)(2,1)} %param.27) | copy-start | bytes 49156
  66.2 11.1 %copy-start.9 = (f32[128]{0:T(128)S(1)}, f32[128]{0:T(128)}, u32[]{:S(2)}) copy-start(f32[128]{0:T(128)} %param.28) | copy-start | bytes 1540
  66.2 11.2 %copy-start.7 = (f32[2048]{0:T(1024)S(1)}, f32[2048]{0:T(1024)}, u32[]{:S(2)}) copy-start(f32[2048]{0:T(1024)} %param.22) | copy-start | bytes 24580
  66.3 11.6 %collective-permute-start = (bf16[512,384]{1,0:T(8,128)(2,1)S(1)}, bf16[512,384]{1,0:T(8,128)(2,1)S(1)}, u32[]{:S(2)}, u32[]{:S(2)}) collective-permute-start(bf16[512,384]{1,0:T(8,128)(2,1)S(1)} %slice.163), channel_id=1, source_target_pairs={{0,8},{8,16},{16,24},{24,0},{1,9},{9,17},{17,25},{25,1},{2,10},{10... | collective-permute-start | bytes 1179656 | tf_op jit(solution)/shard_map/ppermute | solution.py:135
  69.6 8.5 %collective-permute-start.1 = (bf16[512,384]{1,0:T(8,128)(2,1)S(1)}, bf16[512,384]{1,0:T(8,128)(2,1)S(1)}, u32[]{:S(2)}, u32[]{:S(2)}) collective-permute-start(bf16[512,384]{1,0:T(8,128)(2,1)S(1)} %slice.163), channel_id=1, source_target_pairs={{0,24},{8,0},{16,8},{24,16},{1,25},{9,1},{17,9},{25,17},{2,26},{10... | collective-permute-start | bytes 1179656 | tf_op jit(solution)/shard_map/ppermute | solution.py:135
  73.0 10.0 %collective-permute-start.2 = (bf16[512,384]{1,0:T(8,128)(2,1)S(1)}, bf16[512,384]{1,0:T(8,128)(2,1)S(1)}, u32[]{:S(2)}, u32[]{:S(2)}) collective-permute-start(bf16[512,384]{1,0:T(8,128)(2,1)S(1)} %slice.163), channel_id=1, source_target_pairs={{0,16},{8,24},{16,0},{24,8},{1,17},{9,25},{17,1},{25,9},{2,18},{10... | collective-permute-start | bytes 1179656 | tf_op jit(solution)/shard_map/ppermute | solution.py:135
  77.4 5.6 %copy-start = (f32[384,128]{1,0:T(8,128)S(1)}, f32[384,128]{1,0:T(8,128)}, u32[]{:S(2)}) copy-start(f32[384,128]{1,0:T(8,128)} %extra.1) | copy-start | bytes 589828
  77.4 5.6 %copy-start.1 = (bf16[4,128]{1,0:T(4,128)(2,1)S(1)}, bf16[4,128]{1,0:T(4,128)(2,1)}, u32[]{:S(2)}) copy-start(bf16[4,128]{1,0:T(4,128)(2,1)} %taps.1) | copy-start | bytes 3076
  85.8 19.8 %collective-permute-start.3 = (bf16[192,2048]{1,0:T(8,128)(2,1)S(1)}, bf16[192,2048]{1,0:T(8,128)(2,1)S(1)}, u32[]{:S(2)}, u32[]{:S(2)}) collective-permute-start(bf16[192,2048]{1,0:T(8,128)(2,1)S(1)} %get-tuple-element.58), channel_id=1, source_target_pairs={{0,1},{1,0},{2,3},{3,2},{4,5},{5,4},{6,7},{7,6},{8,9},{9,8},{10,11... | collective-permute-start | bytes 2359304 | tf_op jit(solution)/shard_map/ppermute | solution.py:199
  105.6 5.4 %copy-start.4 = (bf16[512,1408]{1,0:T(8,128)(2,1)S(1)}, bf16[512,1408]{1,0:T(8,128)(2,1)}, u32[]{:S(2)}) copy-start(bf16[512,1408]{1,0:T(8,128)(2,1)} %copy-done.3) | copy-start | bytes 4325380
  106.8 16.1 %all-to-all-start = ((bf16[4,48,2048]{2,1,0:T(8,128)(2,1)}), bf16[4,48,2048]{2,1,0:T(8,128)(2,1)}, u32[]{:S(2)}, u32[]{:S(2)}) async-start(bf16[4,48,2048]{2,1,0:T(8,128)(2,1)} %bitcast.9), calls=%async_computation | async-start | bytes 1572864 | tf_op jit(solution)/shard_map/all_to_all | solution.py:142
  111.0 14.3 %copy-start.8 = (f32[2048]{0:T(1024)S(1)}, f32[2048]{0:T(1024)}, u32[]{:S(2)}) copy-start(f32[2048]{0:T(1024)} %param.31) | copy-start | bytes 24580
  111.1 30.6 %collective-permute-start.4 = (bf16[512,1024]{1,0:T(8,128)(2,1)S(1)}, bf16[512,1024]{1,0:T(8,128)(2,1)S(1)}, u32[]{:S(2)}, u32[]{:S(2)}) collective-permute-start(bf16[512,1024]{1,0:T(8,128)(2,1)S(1)} %slice.164), channel_id=1, source_target_pairs={{0,8},{8,16},{16,24},{24,0},{1,9},{9,17},{17,25},{25,1},{2,10},{10... | collective-permute-start | bytes 3145736 | tf_op jit(solution)/shard_map/ppermute | solution.py:135
  114.2 27.6 %collective-permute-start.5 = (bf16[512,1024]{1,0:T(8,128)(2,1)S(1)}, bf16[512,1024]{1,0:T(8,128)(2,1)S(1)}, u32[]{:S(2)}, u32[]{:S(2)}) collective-permute-start(bf16[512,1024]{1,0:T(8,128)(2,1)S(1)} %slice.164), channel_id=1, source_target_pairs={{0,24},{8,0},{16,8},{24,16},{1,25},{9,1},{17,9},{25,17},{2,26},{10... | collective-permute-start | bytes 3145736 | tf_op jit(solution)/shard_map/ppermute | solution.py:135
  117.6 43.7 %collective-permute-start.6 = (bf16[512,1024]{1,0:T(8,128)(2,1)S(1)}, bf16[512,1024]{1,0:T(8,128)(2,1)}, u32[]{:S(2)}, u32[]{:S(2)}) collective-permute-start(bf16[512,1024]{1,0:T(8,128)(2,1)S(1)} %slice.164), channel_id=1, source_target_pairs={{0,16},{8,24},{16,0},{24,8},{1,17},{9,25},{17,1},{25,9},{2,18},{10... | collective-permute-start | bytes 3145736 | tf_op jit(solution)/shard_map/ppermute | solution.py:135
  165.2 6.0 %collective-permute-start.7 = (bf16[192,2048]{1,0:T(8,128)(2,1)S(1)}, bf16[192,2048]{1,0:T(8,128)(2,1)S(1)}, u32[]{:S(2)}, u32[]{:S(2)}) collective-permute-start(bf16[192,2048]{1,0:T(8,128)(2,1)S(1)} %get-tuple-element.60), channel_id=1, source_target_pairs={{0,1},{1,0},{2,3},{3,2},{4,5},{5,4},{6,7},{7,6},{8,9},{9,8},{10,11... | collective-permute-start | bytes 2359304 | tf_op jit(solution)/shard_map/ppermute | solution.py:199

commit v3 on v2

--- a/solution.py
+++ b/solution.py
@@ -10,6 +10,8 @@
 decay_rate_scale = 8.0
 wire_scale = 65536.0
 row_scale = 512.0
+narrow_steps = (2, 1, 3)
+wide_steps = (1, 3, 2)
 
 
 def ring(count, step):
@@ -36,7 +38,7 @@
 
 def assemble(pieces, whole):
     me = lax.axis_index("y")
-    for step, piece in zip((0, 1, 3, 2), pieces):
+    for step, piece in enumerate(pieces):
         whole[:, lax.rem(me + 4 - step, 4)] = piece[...]
 
 
@@ -128,19 +130,26 @@
     )(*operands, *pieces)
 
 
-def y_pieces(rows, height):
-    count = lax.axis_size("y")
-    pieces = [rows]
-    for step in (1, count - 1, 2):
-        pieces.append(lax.ppermute(rows, "y", ring(count, step)))
-    return [piece.reshape(-1, height, rows.shape[1]) for piece in pieces]
-
-
-def x_summed(rows):
+def y_pieces(rows, steps, height):
+    pieces = {0: rows}
+    for step in steps:
+        pieces[step] = lax.ppermute(rows, "y", ring(lax.axis_size("y"), step))
+    return [pieces[k].reshape(-1, height, rows.shape[1]) for k in range(len(pieces))]
+
+
+def x_spread(rows):
     count = lax.axis_size("x")
     tiles = rows.reshape(count, rows.shape[0] // count, rows.shape[1])
-    arrived = lax.all_to_all(tiles, "x", 0, 0, tiled=True)
-    return arrived.astype(jnp.float32).sum(axis=0)
+    return lax.all_to_all(tiles, "x", 0, 0, tiled=True)
+
+
+def settle_kernel(arrived, own_rows, scale, residual, sent):
+    total = arrived[0].astype(jnp.float32)
+    for k in range(1, arrived.shape[0]):
+        total = total + arrived[k].astype(jnp.float32)
+    rows = (own_rows[...].astype(jnp.float32) + total).astype(jnp.bfloat16)
+    residual[...] = rows
+    sent[...] = rms_scaled(rows, scale[...]) * jnp.asarray(row_scale, jnp.bfloat16)
 
 
 def added(left, right):
@@ -181,22 +190,27 @@
         out_shape=jax.ShapeDtypeStruct((height, sum(k.shape[1] for k in matrices)), jnp.bfloat16),
         in_specs=in_vmem(len(matrices)),
         out_specs=in_vmem(1)[0],
+        compiler_params=pltpu.CompilerParams(vmem_limit_bytes=4 << 20),
         name="join",
     )(*matrices)
     z_rows = lax.all_gather(joined.astype(jnp.float16), "z", axis=0, tiled=True)
     z_rows = (z_rows.astype(jnp.float32) * (1.0 / wire_scale)).astype(jnp.bfloat16)
-    first = y_pieces(z_rows[:, : 3 * channels], height)
-    second = y_pieces(z_rows[:, 3 * channels :], height)
+    first = y_pieces(z_rows[:, : 3 * channels], narrow_steps, height)
+    second = y_pieces(z_rows[:, 3 * channels :], wide_steps, height)
 
     normed = rms_scaled(tokens, first_norm_scale)
+    own_rows = lax.dynamic_slice_in_dim(
+        tokens, (x_index * c_count + c_index) * own_count, own_count, 0
+    )
+    normed, own_rows = lax.optimization_barrier((normed, own_rows))
     diagonal = jnp.zeros((2, channels // 2, 2, 2, channels // 2), jnp.bfloat16)
     for group in range(2):
         diagonal = diagonal.at[group, :, 0, group].set(recurrence_gate_blocks[group])
         diagonal = diagonal.at[group, :, 1, group].set(input_gate_blocks[group])
     decay = (decay_rate_scale * jax.nn.log_sigmoid(base_decay_logits))[None]
 
-    def given_summed(given, kept):
-        return x_summed(added(kept, lax.ppermute(given, "c", ring(c_count, 1))))
+    def exchanged(given, kept):
+        return x_spread(added(kept, lax.ppermute(given, "c", ring(c_count, 1))))
 
     by_core = (x_count, c_count, own_count)
     given, kept = mixed(
@@ -206,13 +220,16 @@
         (*by_core, channels),
         6 * positions * width * channels,
     )
-    mixer_out = given_summed(given, kept)
-    own_rows = lax.dynamic_slice_in_dim(
-        tokens, (x_index * c_count + c_index) * own_count, own_count, 0
-    )
-    residual = (own_rows.astype(jnp.float32) + mixer_out).astype(jnp.bfloat16)
-    normed_mid = rms_scaled(residual, second_norm_scale)
-    sent = (normed_mid.astype(jnp.float32) * row_scale).astype(jnp.float16)
+    rows_out = jax.ShapeDtypeStruct((own_count, width), jnp.bfloat16)
+    residual, sent = pl.pallas_call(
+        settle_kernel,
+        out_shape=(rows_out, rows_out),
+        in_specs=in_vmem(3),
+        out_specs=tuple(in_vmem(2)),
+        compiler_params=pltpu.CompilerParams(vmem_limit_bytes=8 << 20),
+        name="settle",
+    )(exchanged(given, kept), own_rows, second_norm_scale[None])
+    sent = sent.astype(jnp.float16)
     arrived = lax.all_gather(sent, ("x", "c"), axis=0, tiled=True)
     rows = (arrived.astype(jnp.float32) * (1.0 / row_scale)).astype(jnp.bfloat16)
     given, kept = mixed(
@@ -222,7 +239,7 @@
         (*by_core, mixer_up_matrix.shape[1]),
         4 * positions * width * mixer_up_matrix.shape[1],
     )
-    channel_sum = given_summed(given, kept)
+    channel_sum = exchanged(given, kept).astype(jnp.float32).sum(axis=0)
     return (residual.astype(jnp.float32) + channel_sum).astype(jnp.bfloat16)
 
 

time: 189 us -> 196 us (1.037)
  local copies, waits for them, and re-layouts: 0.56 us -> 7.15 us
    unnamed x20 -> x26, local copies, waits for them, and re-layouts: 0.06 us -> 4.46 us
    all_to_all x1, waiting for transfers between devices: 2.85 us -> 0.01 us  [x_spread(): return lax.all_to_all(tiles, 'x', 0, 0, tiled=True)]
    ppermute x8, waiting for transfers between devices: 28.5 us -> 30.8 us  [the longest x6 27.1 us: y_pieces(): pieces[step] = lax.ppermute(rows, 'y', ring(lax.axis_size('y'), step))]
    slice x2, local copies, waits for them, and re-layouts: 0.17 us -> 2.34 us  [the longest x1 1.29 us: layer(): second = y_pieces(z_rows[:, 3 * channels:], wide_steps, height)]
where the time goes in v3:
time: 196 us; the launch traced here: 194 us
  blocking collectives  95.9 us (49%)
  starting transfers between devices  46.8 us (24%)
  waiting for transfers between devices  30.8 us (16%)
  Pallas kernels  7.2 us (4%)
  local copies, waits for them, and re-layouts  7.15 us (4%)
  other arithmetic  6.27 us (3%)
    all_gather x1, blocking collectives, layer(): z_rows = lax.all_gather(joined.astype(jnp.float16), 'z', axis=0, tiled=True)  63.7 us
    ppermute x6, waiting for transfers between devices, y_pieces(): pieces[step] = lax.ppermute(rows, 'y', ring(lax.axis_size('y'), step))  27.1 us
    ppermute x6, starting transfers between devices, y_pieces(): pieces[step] = lax.ppermute(rows, 'y', ring(lax.axis_size('y'), step))  21.4 us
    ppermute x2, starting transfers between devices, exchanged(): return x_spread(added(kept, lax.ppermute(given, 'c', ring(c_count, 1))))  21.3 us
    all_gather x1, blocking collectives, layer(): arrived = lax.all_gather(sent, ('x', 'c'), axis=0, tiled=True)  16.7 us
    all_to_all x1, blocking collectives, x_spread(): return lax.all_to_all(tiles, 'x', 0, 0, tiled=True)  15.5 us
    pallas_call x2, Pallas kernels, mixed(): pl.pallas_call(kernel, out_shape=(half, half), in_specs=in_vmem(len(opera...  6.91 us
    unnamed x26, local copies, waits for them, and re-layouts  4.46 us
  transfers between devices with their start and end apart: 9, of which 6 were waited for; matrix products, arithmetic and copies ran while one was open for 2% of the time, Pallas kernels for 0%

profile of v3, /device:TPU:1, one launch (start us, length us, event | category | flops | bytes accessed | tf_op | source)
XLA Modules:
  0.0 194.4 jit_solution(4097642155629615777)
XLA Ops:
  0.0 0.7 copy-done.1
  0.7 0.7 copy-done.2
  1.4 0.7 copy-done.4
  2.1 0.7 copy-done.5
  2.8 0.7 copy-done.6
  3.5 63.7 %all-gather.2 = f16[512,1408]{1,0:T(8,128)(2,1)S(1)} all-gather(f16[16,1408]{1,0:T(8,128)(2,1)S(1)} %convert_element_type.53), channel_id=1, replica_groups=mesh['z'=32,'y'=4,'x'=4,'c'=2] {'z'}, dimensions={0}, use_global_device_ids=true | all-gather | bytes 1486848 | tf_op jit(solution)/shard_map/all_gather | solution.py:196
  67.2 1.4 multiply_convert_fusion.1
  68.6 1.0 slice.163
  69.7 3.2 %collective-permute-start = (bf16[512,384]{1,0:T(8,128)(2,1)S(1)}, bf16[512,384]{1,0:T(8,128)(2,1)S(1)}, u32[]{:S(2)}, u32[]{:S(2)}) collective-permute-start(bf16[512,384]{1,0:T(8,128)(2,1)S(1)} %slice.163), channel_id=1, source_target_pairs={{0,8},{8,16},{16,24},{24,0},{1,9},{9,17},{17,25},{25,1},{2,10},{10... | collective-permute-start | bytes 1179656 | tf_op jit(solution)/shard_map/ppermute | solution.py:136
  72.9 4.5 %collective-permute-start.1 = (bf16[512,384]{1,0:T(8,128)(2,1)S(1)}, bf16[512,384]{1,0:T(8,128)(2,1)S(1)}, u32[]{:S(2)}, u32[]{:S(2)}) collective-permute-start(bf16[512,384]{1,0:T(8,128)(2,1)S(1)} %slice.163), channel_id=1, source_target_pairs={{0,16},{8,24},{16,0},{24,8},{1,17},{9,25},{17,1},{25,9},{2,18},{10... | collective-permute-start | bytes 1179656 | tf_op jit(solution)/shard_map/ppermute | solution.py:136
  77.4 3.0 %collective-permute-start.2 = (bf16[512,384]{1,0:T(8,128)(2,1)S(1)}, bf16[512,384]{1,0:T(8,128)(2,1)S(1)}, u32[]{:S(2)}, u32[]{:S(2)}) collective-permute-start(bf16[512,384]{1,0:T(8,128)(2,1)S(1)} %slice.163), channel_id=1, source_target_pairs={{0,24},{8,0},{16,8},{24,16},{1,25},{9,1},{17,9},{25,17},{2,26},{10... | collective-permute-start | bytes 1179656 | tf_op jit(solution)/shard_map/ppermute | solution.py:136
  80.4 0.0 copy-done.8
  80.4 0.4 fusion
  80.8 0.0 copy-done.11
  80.8 0.0 copy-start.9
  80.9 0.0 copy-start.10
  80.9 0.0 copy-start.12
  80.9 0.0 copy-start.7
  80.9 1.8 fusion.2.normed
  82.8 0.1 copy.14
  83.0 0.1 reshape.216.gates
  83.2 0.0 collective-permute-done
  83.2 1.7 collective-permute-done.1
  84.9 1.3 collective-permute-done.2
  86.2 0.9 copy-done
  87.1 2.7 %shard_map.127 = (bf16[192,2048]{1,0:T(8,128)(2,1)S(1)}, bf16[192,2048]{1,0:T(8,128)(2,1)S(1)}) custom-call(bf16[384,2048]{1,0:T(8,128)(2,1)S(1)} %fusion.2.normed, bf16[4,128]{1,0:T(4,128)(2,1)S(1)} %copy-done.7, bf16[128,256]{1,0:T(8,128)(2,1)S(1)} %reshape.216.gates, f32[1,128]{1,0:T(1,128)S(1)} %multiply_bitcast_fusion.decay, f32[384,128]{1,0:T(8,128)S(1)} %copy-done, ...), custom_call_target="tpu_custom_call" | custom-call | flops 603979776 | bytes 8388608 | tf_op jit(solution)/shard_map/pallas_call | solution.py:119
  89.8 17.7 %collective-permute-start.3 = (bf16[192,2048]{1,0:T(8,128)(2,1)S(1)}, bf16[192,2048]{1,0:T(8,128)(2,1)S(1)}, u32[]{:S(2)}, u32[]{:S(2)}) collective-permute-start(bf16[192,2048]{1,0:T(8,128)(2,1)S(1)} %get-tuple-element.63), channel_id=1, source_target_pairs={{0,1},{1,0},{2,3},{3,2},{4,5},{5,4},{6,7},{7,6},{8,9},{9,8},{10,11... | collective-permute-start | bytes 2359304 | tf_op jit(solution)/shard_map/ppermute | solution.py:213
  107.6 1.9 collective-permute-done.3
  109.5 1.2 add_convert_fusion.1
  110.6 4.1 %all-to-all-start = ((bf16[4,48,2048]{2,1,0:T(8,128)(2,1)}), bf16[4,48,2048]{2,1,0:T(8,128)(2,1)S(1)}, u32[]{:S(2)}, u32[]{:S(2)}) async-start(bf16[4,48,2048]{2,1,0:T(8,128)(2,1)} %bitcast.9), calls=%async_computation | async-start | bytes 1572864 | tf_op jit(solution)/shard_map/all_to_all | solution.py:143
  114.8 1.3 slice.164
  116.1 4.1 %collective-permute-start.4 = (bf16[512,1024]{1,0:T(8,128)(2,1)S(1)}, bf16[512,1024]{1,0:T(8,128)(2,1)S(1)}, u32[]{:S(2)}, u32[]{:S(2)}) collective-permute-start(bf16[512,1024]{1,0:T(8,128)(2,1)S(1)} %slice.164), channel_id=1, source_target_pairs={{0,8},{8,16},{16,24},{24,0},{1,9},{9,17},{17,25},{25,1},{2,10},{10... | collective-permute-start | bytes 3145736 | tf_op jit(solution)/shard_map/ppermute | solution.py:136
  120.2 3.2 %collective-permute-start.5 = (bf16[512,1024]{1,0:T(8,128)(2,1)S(1)}, bf16[512,1024]{1,0:T(8,128)(2,1)}, u32[]{:S(2)}, u32[]{:S(2)}) collective-permute-start(bf16[512,1024]{1,0:T(8,128)(2,1)S(1)} %slice.164), channel_id=1, source_target_pairs={{0,16},{8,24},{16,0},{24,8},{1,17},{9,25},{17,1},{25,9},{2,18},{10... | collective-permute-start | bytes 3145736 | tf_op jit(solution)/shard_map/ppermute | solution.py:136
  123.4 3.4 %collective-permute-start.6 = (bf16[512,1024]{1,0:T(8,128)(2,1)S(1)}, bf16[512,1024]{1,0:T(8,128)(2,1)}, u32[]{:S(2)}, u32[]{:S(2)}) collective-permute-start(bf16[512,1024]{1,0:T(8,128)(2,1)S(1)} %slice.164), channel_id=1, source_target_pairs={{0,24},{8,0},{16,8},{24,16},{1,25},{9,1},{17,9},{25,17},{2,26},{10... | collective-permute-start | bytes 3145736 | tf_op jit(solution)/shard_map/ppermute | solution.py:136
  126.8 0.0 all-to-all-done.arrived
  126.8 0.3 settle.1
  127.1 16.7 %all-gather.3 = f16[384,2048]{1,0:T(8,128)(2,1)S(1)} all-gather(f16[48,2048]{1,0:T(8,128)(2,1)S(1)} %convert_element_type.60), channel_id=1, replica_groups=mesh['z'=32,'y'=4,'x'=4,'c'=2] {'x','c'}, dimensions={0}, use_global_device_ids=true | all-gather | bytes 1769472 | tf_op jit(solution)/shard_map/all_gather | solution.py:233
  143.8 0.3 multiply_convert_fusion.rows
  144.2 0.0 collective-permute-done.4
  144.2 22.4 %collective-permute-done.5 = bf16[512,1024]{1,0:T(8,128)(2,1)} collective-permute-done((bf16[512,1024]{1,0:T(8,128)(2,1)S(1)}, bf16[512,1024]{1,0:T(8,128)(2,1)}, u32[]{:S(2)}, u32[]{:S(2)}) %collective-permute-start.5) | collective-permute-done | bytes 1048608 | tf_op jit(solution)/shard_map/ppermute | solution.py:136
  166.6 1.6 collective-permute-done.6
  168.2 4.2 %shard_map.128 = (bf16[192,2048]{1,0:T(8,128)(2,1)S(1)}, bf16[192,2048]{1,0:T(8,128)(2,1)S(1)}) custom-call(bf16[384,2048]{1,0:T(8,128)(2,1)S(1)} %multiply_convert_fusion.rows, bf16[32,16,1024]{2,1,0:T(8,128)(2,1)S(1)} %bitcast.22, bf16[32,16,1024]{2,1,0:T(8,128)(2,1)S(1)} %bitcast.27, bf16[32,16,1024]{2,1,0:T(8,128)(2,1)} %bitcast.13.p2, ...), custom_call_target="tpu_custom_call" | custom-call | flops 1610612736 | bytes 8388608 | tf_op jit(solution)/shard_map/pallas_call | solution.py:119
  172.4 3.6 %collective-permute-start.7 = (bf16[192,2048]{1,0:T(8,128)(2,1)S(1)}, bf16[192,2048]{1,0:T(8,128)(2,1)S(1)}, u32[]{:S(2)}, u32[]{:S(2)}) collective-permute-start(bf16[192,2048]{1,0:T(8,128)(2,1)S(1)} %get-tuple-element.68), channel_id=1, source_target_pairs={{0,1},{1,0},{2,3},{3,2},{4,5},{5,4},{6,7},{7,6},{8,9},{9,8},{10,11... | collective-permute-start | bytes 2359304 | tf_op jit(solution)/shard_map/ppermute | solution.py:213
  176.0 1.9 collective-permute-done.7
  177.9 0.3 add_convert_fusion
  178.1 15.5 %all_to_all.10 = bf16[4,48,2048]{2,1,0:T(8,128)(2,1)S(1)} all-to-all(bf16[4,48,2048]{2,1,0:T(8,128)(2,1)S(1)} %bitcast.28), channel_id=1, replica_groups=mesh['z'=32,'y'=4,'x'=4,'c'=2] {'x'}, dimensions={0} | all-to-all | bytes 1572864 | tf_op jit(solution)/shard_map/all_to_all | solution.py:143
  193.6 0.1 convert_reduce_fusion
  193.7 0.7 add_convert_fusion.2
  (25 shorter events, 0.2 us)
Async XLA Ops:
  0.0 0.7 copy-start.1
  0.7 0.7 copy-start.2
  1.4 0.7 copy-start.4
  2.1 0.7 copy-start.5
  2.8 0.7 copy-start.6
  67.2 13.2 %copy-start.8 = (bf16[384,2048]{1,0:T(8,128)(2,1)S(1)}, bf16[384,2048]{1,0:T(8,128)(2,1)}, u32[]{:S(2)}) copy-start(bf16[384,2048]{1,0:T(8,128)(2,1)} %param.21) | copy-start | bytes 4718596
  68.6 12.2 %copy-start.11 = (f32[2048]{0:T(1024)S(1)}, f32[2048]{0:T(1024)}, u32[]{:S(2)}) copy-start(f32[2048]{0:T(1024)} %param.22) | copy-start | bytes 24580
  69.7 13.5 %collective-permute-start = (bf16[512,384]{1,0:T(8,128)(2,1)S(1)}, bf16[512,384]{1,0:T(8,128)(2,1)S(1)}, u32[]{:S(2)}, u32[]{:S(2)}) collective-permute-start(bf16[512,384]{1,0:T(8,128)(2,1)S(1)} %slice.163), channel_id=1, source_target_pairs={{0,8},{8,16},{16,24},{24,0},{1,9},{9,17},{17,25},{25,1},{2,10},{10... | collective-permute-start | bytes 1179656 | tf_op jit(solution)/shard_map/ppermute | solution.py:136
  72.9 12.0 %collective-permute-start.1 = (bf16[512,384]{1,0:T(8,128)(2,1)S(1)}, bf16[512,384]{1,0:T(8,128)(2,1)S(1)}, u32[]{:S(2)}, u32[]{:S(2)}) collective-permute-start(bf16[512,384]{1,0:T(8,128)(2,1)S(1)} %slice.163), channel_id=1, source_target_pairs={{0,16},{8,24},{16,0},{24,8},{1,17},{9,25},{17,1},{25,9},{2,18},{10... | collective-permute-start | bytes 1179656 | tf_op jit(solution)/shard_map/ppermute | solution.py:136
  77.4 8.8 %collective-permute-start.2 = (bf16[512,384]{1,0:T(8,128)(2,1)S(1)}, bf16[512,384]{1,0:T(8,128)(2,1)S(1)}, u32[]{:S(2)}, u32[]{:S(2)}) collective-permute-start(bf16[512,384]{1,0:T(8,128)(2,1)S(1)} %slice.163), channel_id=1, source_target_pairs={{0,24},{8,0},{16,8},{24,16},{1,25},{9,1},{17,9},{25,17},{2,26},{10... | collective-permute-start | bytes 1179656 | tf_op jit(solution)/shard_map/ppermute | solution.py:136
  80.8 1.9 copy-start.9
  80.9 1.9 copy-start.10
  80.9 2.3 %copy-start.12 = (f32[128]{0:T(128)S(1)}, f32[128]{0:T(128)}, u32[]{:S(2)}) copy-start(f32[128]{0:T(128)} %param.28) | copy-start | bytes 1540
  80.9 5.3 %copy-start.7 = (bf16[4,128]{1,0:T(4,128)(2,1)S(1)}, bf16[4,128]{1,0:T(4,128)(2,1)}, u32[]{:S(2)}) copy-start(bf16[4,128]{1,0:T(4,128)(2,1)} %taps.1) | copy-start | bytes 3076
  86.2 0.9 copy-start
  89.8 19.6 %collective-permute-start.3 = (bf16[192,2048]{1,0:T(8,128)(2,1)S(1)}, bf16[192,2048]{1,0:T(8,128)(2,1)S(1)}, u32[]{:S(2)}, u32[]{:S(2)}) collective-permute-start(bf16[192,2048]{1,0:T(8,128)(2,1)S(1)} %get-tuple-element.63), channel_id=1, source_target_pairs={{0,1},{1,0},{2,3},{3,2},{4,5},{5,4},{6,7},{7,6},{8,9},{9,8},{10,11... | collective-permute-start | bytes 2359304 | tf_op jit(solution)/shard_map/ppermute | solution.py:213
  110.6 16.1 %copy-start.3 = (f32[2048]{0:T(1024)S(1)}, f32[2048]{0:T(1024)}, u32[]{:S(2)}) copy-start(f32[2048]{0:T(1024)} %param.31) | copy-start | bytes 24580
  110.6 16.1 %all-to-all-start = ((bf16[4,48,2048]{2,1,0:T(8,128)(2,1)}), bf16[4,48,2048]{2,1,0:T(8,128)(2,1)S(1)}, u32[]{:S(2)}, u32[]{:S(2)}) async-start(bf16[4,48,2048]{2,1,0:T(8,128)(2,1)} %bitcast.9), calls=%async_computation | async-start | bytes 1572864 | tf_op jit(solution)/shard_map/all_to_all | solution.py:143
  116.1 28.1 %collective-permute-start.4 = (bf16[512,1024]{1,0:T(8,128)(2,1)S(1)}, bf16[512,1024]{1,0:T(8,128)(2,1)S(1)}, u32[]{:S(2)}, u32[]{:S(2)}) collective-permute-start(bf16[512,1024]{1,0:T(8,128)(2,1)S(1)} %slice.164), channel_id=1, source_target_pairs={{0,8},{8,16},{16,24},{24,0},{1,9},{9,17},{17,25},{25,1},{2,10},{10... | collective-permute-start | bytes 3145736 | tf_op jit(solution)/shard_map/ppermute | solution.py:136
  120.2 46.4 %collective-permute-start.5 = (bf16[512,1024]{1,0:T(8,128)(2,1)S(1)}, bf16[512,1024]{1,0:T(8,128)(2,1)}, u32[]{:S(2)}, u32[]{:S(2)}) collective-permute-start(bf16[512,1024]{1,0:T(8,128)(2,1)S(1)} %slice.164), channel_id=1, source_target_pairs={{0,16},{8,24},{16,0},{24,8},{1,17},{9,25},{17,1},{25,9},{2,18},{10... | collective-permute-start | bytes 3145736 | tf_op jit(solution)/shard_map/ppermute | solution.py:136
  123.4 44.8 %collective-permute-start.6 = (bf16[512,1024]{1,0:T(8,128)(2,1)S(1)}, bf16[512,1024]{1,0:T(8,128)(2,1)}, u32[]{:S(2)}, u32[]{:S(2)}) collective-permute-start(bf16[512,1024]{1,0:T(8,128)(2,1)S(1)} %slice.164), channel_id=1, source_target_pairs={{0,24},{8,0},{16,8},{24,16},{1,25},{9,1},{17,9},{25,17},{2,26},{10... | collective-permute-start | bytes 3145736 | tf_op jit(solution)/shard_map/ppermute | solution.py:136
  172.4 5.5 %collective-permute-start.7 = (bf16[192,2048]{1,0:T(8,128)(2,1)S(1)}, bf16[192,2048]{1,0:T(8,128)(2,1)S(1)}, u32[]{:S(2)}, u32[]{:S(2)}) collective-permute-start(bf16[192,2048]{1,0:T(8,128)(2,1)S(1)} %get-tuple-element.68), channel_id=1, source_target_pairs={{0,1},{1,0},{2,3},{3,2},{4,5},{5,4},{6,7},{7,6},{8,9},{9,8},{10,11... | collective-permute-start | bytes 2359304 | tf_op jit(solution)/shard_map/ppermute | solution.py:213

commit v4 on v3

--- a/solution.py
+++ b/solution.py
@@ -10,8 +10,8 @@
 decay_rate_scale = 8.0
 wire_scale = 65536.0
 row_scale = 512.0
-narrow_steps = (2, 1, 3)
-wide_steps = (1, 3, 2)
+narrow_steps = (2, 3, 1)
+wide_steps = (3, 1, 2)
 
 
 def ring(count, step):
@@ -190,7 +190,6 @@
         out_shape=jax.ShapeDtypeStruct((height, sum(k.shape[1] for k in matrices)), jnp.bfloat16),
         in_specs=in_vmem(len(matrices)),
         out_specs=in_vmem(1)[0],
-        compiler_params=pltpu.CompilerParams(vmem_limit_bytes=4 << 20),
         name="join",
     )(*matrices)
     z_rows = lax.all_gather(joined.astype(jnp.float16), "z", axis=0, tiled=True)
@@ -210,7 +209,9 @@
     decay = (decay_rate_scale * jax.nn.log_sigmoid(base_decay_logits))[None]
 
     def exchanged(given, kept):
-        return x_spread(added(kept, lax.ppermute(given, "c", ring(c_count, 1))))
+        taken = lax.ppermute(given, "c", ring(c_count, 1))
+        both = added(kept, taken)
+        return x_spread(both)
 
     by_core = (x_count, c_count, own_count)
     given, kept = mixed(

time: 196 us -> 195 us (level)
  local copies, waits for them, and re-layouts: 7.15 us -> 3.66 us
    unnamed x26 -> x16, local copies, waits for them, and re-layouts: 4.46 us -> 0.96 us
where the time goes in v4:
time: 195 us; the launch traced here: 193 us
  blocking collectives  95.9 us (49%)
  starting transfers between devices  46.8 us (24%)
  waiting for transfers between devices  30.8 us (16%)
  Pallas kernels  8.6 us (4%)
  other arithmetic  7.05 us (4%)
  local copies, waits for them, and re-layouts  3.66 us (2%)
    all_gather x1, blocking collectives, layer(): z_rows = lax.all_gather(joined.astype(jnp.float16), 'z', axis=0, tiled=True)  63.7 us
    ppermute x6, waiting for transfers between devices, y_pieces(): pieces[step] = lax.ppermute(rows, 'y', ring(lax.axis_size('y'), step))  27.1 us
    ppermute x6, starting transfers between devices, y_pieces(): pieces[step] = lax.ppermute(rows, 'y', ring(lax.axis_size('y'), step))  21.4 us
    ppermute x2, starting transfers between devices, exchanged(): taken = lax.ppermute(given, 'c', ring(c_count, 1))  21.3 us
    all_gather x1, blocking collectives, layer(): arrived = lax.all_gather(sent, ('x', 'c'), axis=0, tiled=True)  16.7 us
    all_to_all x1, blocking collectives, x_spread(): return lax.all_to_all(tiles, 'x', 0, 0, tiled=True)  15.5 us
    pallas_call x2, Pallas kernels, mixed(): pl.pallas_call(kernel, out_shape=(half, half), in_specs=in_vmem(len(opera...  6.91 us
    all_to_all x1, starting transfers between devices, x_spread(): return lax.all_to_all(tiles, 'x', 0, 0, tiled=True)  4.14 us
  transfers between devices with their start and end apart: 9, of which 6 were waited for; matrix products, arithmetic and copies ran while one was open for 2% of the time, Pallas kernels for 0%

profile of v4, /device:TPU:1, one launch (start us, length us, event | category | flops | bytes accessed | tf_op | source)
XLA Modules:
  0.0 193.1 jit_solution(6198476467107817061)
XLA Ops:
  0.0 1.4 join.1
  1.4 0.8 convert_element_type.53
  2.2 63.7 %all-gather.2 = f16[512,1408]{1,0:T(8,128)(2,1)S(1)} all-gather(f16[16,1408]{1,0:T(8,128)(2,1)S(1)} %convert_element_type.53), channel_id=1, replica_groups=mesh['z'=32,'y'=4,'x'=4,'c'=2] {'z'}, dimensions={0}, use_global_device_ids=true | all-gather | bytes 1486848 | tf_op jit(solution)/shard_map/all_gather | solution.py:195
  65.9 1.4 multiply_convert_fusion.1
  67.3 1.0 slice.163
  68.3 3.2 %collective-permute-start = (bf16[512,384]{1,0:T(8,128)(2,1)S(1)}, bf16[512,384]{1,0:T(8,128)(2,1)S(1)}, u32[]{:S(2)}, u32[]{:S(2)}) collective-permute-start(bf16[512,384]{1,0:T(8,128)(2,1)S(1)} %slice.163), channel_id=1, source_target_pairs={{0,8},{8,16},{16,24},{24,0},{1,9},{9,17},{17,25},{25,1},{2,10},{10... | collective-permute-start | bytes 1179656 | tf_op jit(solution)/shard_map/ppermute | solution.py:136
  71.6 4.5 %collective-permute-start.1 = (bf16[512,384]{1,0:T(8,128)(2,1)S(1)}, bf16[512,384]{1,0:T(8,128)(2,1)S(1)}, u32[]{:S(2)}, u32[]{:S(2)}) collective-permute-start(bf16[512,384]{1,0:T(8,128)(2,1)S(1)} %slice.163), channel_id=1, source_target_pairs={{0,16},{8,24},{16,0},{24,8},{1,17},{9,25},{17,1},{25,9},{2,18},{10... | collective-permute-start | bytes 1179656 | tf_op jit(solution)/shard_map/ppermute | solution.py:136
  76.1 3.0 %collective-permute-start.2 = (bf16[512,384]{1,0:T(8,128)(2,1)S(1)}, bf16[512,384]{1,0:T(8,128)(2,1)S(1)}, u32[]{:S(2)}, u32[]{:S(2)}) collective-permute-start(bf16[512,384]{1,0:T(8,128)(2,1)S(1)} %slice.163), channel_id=1, source_target_pairs={{0,24},{8,0},{16,8},{24,16},{1,25},{9,1},{17,9},{25,17},{2,26},{10... | collective-permute-start | bytes 1179656 | tf_op jit(solution)/shard_map/ppermute | solution.py:136
  79.1 0.0 copy-done.3
  79.1 0.4 fusion
  79.5 0.0 copy-done.6
  79.5 0.0 copy-start.4
  79.5 0.0 copy-start.5
  79.6 0.0 copy-start.7
  79.6 0.0 copy-start.2
  79.6 1.8 fusion.2.normed
  81.4 0.0 copy-done.4
  81.5 0.0 copy-done.5
  81.5 0.1 copy.14
  81.7 0.1 reshape.216.gates
  81.8 0.0 copy-done.7
  81.8 0.0 collective-permute-done
  81.9 1.7 collective-permute-done.1
  83.5 1.3 collective-permute-done.2
  84.9 0.9 copy-done
  85.8 2.7 %shard_map.127 = (bf16[192,2048]{1,0:T(8,128)(2,1)S(1)}, bf16[192,2048]{1,0:T(8,128)(2,1)S(1)}) custom-call(bf16[384,2048]{1,0:T(8,128)(2,1)S(1)} %fusion.2.normed, bf16[4,128]{1,0:T(4,128)(2,1)S(1)} %copy-done.2, bf16[128,256]{1,0:T(8,128)(2,1)S(1)} %reshape.216.gates, f32[1,128]{1,0:T(1,128)S(1)} %multiply_bitcast_fusion.decay, f32[384,128]{1,0:T(8,128)S(1)} %copy-done, ...), custom_call_target="tpu_custom_call" | custom-call | flops 603979776 | bytes 8388608 | tf_op jit(solution)/shard_map/pallas_call | solution.py:119
  88.5 17.7 %collective-permute-start.3 = (bf16[192,2048]{1,0:T(8,128)(2,1)S(1)}, bf16[192,2048]{1,0:T(8,128)(2,1)S(1)}, u32[]{:S(2)}, u32[]{:S(2)}) collective-permute-start(bf16[192,2048]{1,0:T(8,128)(2,1)S(1)} %get-tuple-element.63), channel_id=1, source_target_pairs={{0,1},{1,0},{2,3},{3,2},{4,5},{5,4},{6,7},{7,6},{8,9},{9,8},{10,11... | collective-permute-start | bytes 2359304 | tf_op jit(solution)/shard_map/ppermute | solution.py:212
  106.3 1.9 collective-permute-done.3
  108.2 1.2 add_convert_fusion.1
  109.3 4.1 %all-to-all-start = ((bf16[4,48,2048]{2,1,0:T(8,128)(2,1)}), bf16[4,48,2048]{2,1,0:T(8,128)(2,1)S(1)}, u32[]{:S(2)}, u32[]{:S(2)}) async-start(bf16[4,48,2048]{2,1,0:T(8,128)(2,1)} %bitcast.9), calls=%async_computation | async-start | bytes 1572864 | tf_op jit(solution)/shard_map/all_to_all | solution.py:143
  113.5 1.3 slice.164
  114.8 4.1 %collective-permute-start.4 = (bf16[512,1024]{1,0:T(8,128)(2,1)S(1)}, bf16[512,1024]{1,0:T(8,128)(2,1)S(1)}, u32[]{:S(2)}, u32[]{:S(2)}) collective-permute-start(bf16[512,1024]{1,0:T(8,128)(2,1)S(1)} %slice.164), channel_id=1, source_target_pairs={{0,8},{8,16},{16,24},{24,0},{1,9},{9,17},{17,25},{25,1},{2,10},{10... | collective-permute-start | bytes 3145736 | tf_op jit(solution)/shard_map/ppermute | solution.py:136
  118.9 3.2 %collective-permute-start.5 = (bf16[512,1024]{1,0:T(8,128)(2,1)S(1)}, bf16[512,1024]{1,0:T(8,128)(2,1)}, u32[]{:S(2)}, u32[]{:S(2)}) collective-permute-start(bf16[512,1024]{1,0:T(8,128)(2,1)S(1)} %slice.164), channel_id=1, source_target_pairs={{0,16},{8,24},{16,0},{24,8},{1,17},{9,25},{17,1},{25,9},{2,18},{10... | collective-permute-start | bytes 3145736 | tf_op jit(solution)/shard_map/ppermute | solution.py:136
  122.1 3.4 %collective-permute-start.6 = (bf16[512,1024]{1,0:T(8,128)(2,1)S(1)}, bf16[512,1024]{1,0:T(8,128)(2,1)}, u32[]{:S(2)}, u32[]{:S(2)}) collective-permute-start(bf16[512,1024]{1,0:T(8,128)(2,1)S(1)} %slice.164), channel_id=1, source_target_pairs={{0,24},{8,0},{16,8},{24,16},{1,25},{9,1},{17,9},{25,17},{2,26},{10... | collective-permute-start | bytes 3145736 | tf_op jit(solution)/shard_map/ppermute | solution.py:136
  125.4 0.0 all-to-all-done.arrived
  125.5 0.3 settle.1
  125.8 16.7 %all-gather.3 = f16[384,2048]{1,0:T(8,128)(2,1)S(1)} all-gather(f16[48,2048]{1,0:T(8,128)(2,1)S(1)} %convert_element_type.60), channel_id=1, replica_groups=mesh['z'=32,'y'=4,'x'=4,'c'=2] {'x','c'}, dimensions={0}, use_global_device_ids=true | all-gather | bytes 1769472 | tf_op jit(solution)/shard_map/all_gather | solution.py:234
  142.5 0.3 multiply_convert_fusion.rows
  142.8 0.0 collective-permute-done.4
  142.9 22.4 %collective-permute-done.5 = bf16[512,1024]{1,0:T(8,128)(2,1)} collective-permute-done((bf16[512,1024]{1,0:T(8,128)(2,1)S(1)}, bf16[512,1024]{1,0:T(8,128)(2,1)}, u32[]{:S(2)}, u32[]{:S(2)}) %collective-permute-start.5) | collective-permute-done | bytes 1048608 | tf_op jit(solution)/shard_map/ppermute | solution.py:136
  165.3 1.6 collective-permute-done.6
  166.9 4.2 %shard_map.128 = (bf16[192,2048]{1,0:T(8,128)(2,1)S(1)}, bf16[192,2048]{1,0:T(8,128)(2,1)S(1)}) custom-call(bf16[384,2048]{1,0:T(8,128)(2,1)S(1)} %multiply_convert_fusion.rows, bf16[32,16,1024]{2,1,0:T(8,128)(2,1)S(1)} %bitcast.22, bf16[32,16,1024]{2,1,0:T(8,128)(2,1)S(1)} %bitcast.27, bf16[32,16,1024]{2,1,0:T(8,128)(2,1)} %bitcast.13.p2, ...), custom_call_target="tpu_custom_call" | custom-call | flops 1610612736 | bytes 8388608 | tf_op jit(solution)/shard_map/pallas_call | solution.py:119
  171.1 3.6 %collective-permute-start.7 = (bf16[192,2048]{1,0:T(8,128)(2,1)S(1)}, bf16[192,2048]{1,0:T(8,128)(2,1)S(1)}, u32[]{:S(2)}, u32[]{:S(2)}) collective-permute-start(bf16[192,2048]{1,0:T(8,128)(2,1)S(1)} %get-tuple-element.68), channel_id=1, source_target_pairs={{0,1},{1,0},{2,3},{3,2},{4,5},{5,4},{6,7},{7,6},{8,9},{9,8},{10,11... | collective-permute-start | bytes 2359304 | tf_op jit(solution)/shard_map/ppermute | solution.py:212
  174.7 1.9 collective-permute-done.7
  176.6 0.3 add_convert_fusion
  176.8 15.5 %all_to_all.10 = bf16[4,48,2048]{2,1,0:T(8,128)(2,1)S(1)} all-to-all(bf16[4,48,2048]{2,1,0:T(8,128)(2,1)S(1)} %bitcast.28), channel_id=1, replica_groups=mesh['z'=32,'y'=4,'x'=4,'c'=2] {'x'}, dimensions={0} | all-to-all | bytes 1572864 | tf_op jit(solution)/shard_map/all_to_all | solution.py:143
  192.3 0.1 convert_reduce_fusion
  192.4 0.7 add_convert_fusion.2
  (15 shorter events, 0.1 us)
Async XLA Ops:
  65.9 13.2 %copy-start.3 = (bf16[384,2048]{1,0:T(8,128)(2,1)S(1)}, bf16[384,2048]{1,0:T(8,128)(2,1)}, u32[]{:S(2)}) copy-start(bf16[384,2048]{1,0:T(8,128)(2,1)} %param.21) | copy-start | bytes 4718596
  67.3 12.2 %copy-start.6 = (f32[2048]{0:T(1024)S(1)}, f32[2048]{0:T(1024)}, u32[]{:S(2)}) copy-start(f32[2048]{0:T(1024)} %param.22) | copy-start | bytes 24580
  68.3 13.5 %collective-permute-start = (bf16[512,384]{1,0:T(8,128)(2,1)S(1)}, bf16[512,384]{1,0:T(8,128)(2,1)S(1)}, u32[]{:S(2)}, u32[]{:S(2)}) collective-permute-start(bf16[512,384]{1,0:T(8,128)(2,1)S(1)} %slice.163), channel_id=1, source_target_pairs={{0,8},{8,16},{16,24},{24,0},{1,9},{9,17},{17,25},{25,1},{2,10},{10... | collective-permute-start | bytes 1179656 | tf_op jit(solution)/shard_map/ppermute | solution.py:136
  71.6 12.0 %collective-permute-start.1 = (bf16[512,384]{1,0:T(8,128)(2,1)S(1)}, bf16[512,384]{1,0:T(8,128)(2,1)S(1)}, u32[]{:S(2)}, u32[]{:S(2)}) collective-permute-start(bf16[512,384]{1,0:T(8,128)(2,1)S(1)} %slice.163), channel_id=1, source_target_pairs={{0,16},{8,24},{16,0},{24,8},{1,17},{9,25},{17,1},{25,9},{2,18},{10... | collective-permute-start | bytes 1179656 | tf_op jit(solution)/shard_map/ppermute | solution.py:136
  76.1 8.8 %collective-permute-start.2 = (bf16[512,384]{1,0:T(8,128)(2,1)S(1)}, bf16[512,384]{1,0:T(8,128)(2,1)S(1)}, u32[]{:S(2)}, u32[]{:S(2)}) collective-permute-start(bf16[512,384]{1,0:T(8,128)(2,1)S(1)} %slice.163), channel_id=1, source_target_pairs={{0,24},{8,0},{16,8},{24,16},{1,25},{9,1},{17,9},{25,17},{2,26},{10... | collective-permute-start | bytes 1179656 | tf_op jit(solution)/shard_map/ppermute | solution.py:136
  79.5 1.9 copy-start.4
  79.5 1.9 %copy-start.5 = (bf16[2,64,64]{2,1,0:T(8,128)(2,1)S(1)}, bf16[2,64,64]{2,1,0:T(8,128)(2,1)}, u32[]{:S(2)}) copy-start(bf16[2,64,64]{2,1,0:T(8,128)(2,1)} %param.27) | copy-start | bytes 49156
  79.6 2.3 %copy-start.7 = (f32[128]{0:T(128)S(1)}, f32[128]{0:T(128)}, u32[]{:S(2)}) copy-start(f32[128]{0:T(128)} %param.28) | copy-start | bytes 1540
  79.6 5.3 %copy-start.2 = (bf16[4,128]{1,0:T(4,128)(2,1)S(1)}, bf16[4,128]{1,0:T(4,128)(2,1)}, u32[]{:S(2)}) copy-start(bf16[4,128]{1,0:T(4,128)(2,1)} %taps.1) | copy-start | bytes 3076
  84.9 0.9 copy-start
  88.5 19.6 %collective-permute-start.3 = (bf16[192,2048]{1,0:T(8,128)(2,1)S(1)}, bf16[192,2048]{1,0:T(8,128)(2,1)S(1)}, u32[]{:S(2)}, u32[]{:S(2)}) collective-permute-start(bf16[192,2048]{1,0:T(8,128)(2,1)S(1)} %get-tuple-element.63), channel_id=1, source_target_pairs={{0,1},{1,0},{2,3},{3,2},{4,5},{5,4},{6,7},{7,6},{8,9},{9,8},{10,11... | collective-permute-start | bytes 2359304 | tf_op jit(solution)/shard_map/ppermute | solution.py:212
  109.3 16.1 %copy-start.1 = (f32[2048]{0:T(1024)S(1)}, f32[2048]{0:T(1024)}, u32[]{:S(2)}) copy-start(f32[2048]{0:T(1024)} %param.31) | copy-start | bytes 24580
  109.3 16.1 %all-to-all-start = ((bf16[4,48,2048]{2,1,0:T(8,128)(2,1)}), bf16[4,48,2048]{2,1,0:T(8,128)(2,1)S(1)}, u32[]{:S(2)}, u32[]{:S(2)}) async-start(bf16[4,48,2048]{2,1,0:T(8,128)(2,1)} %bitcast.9), calls=%async_computation | async-start | bytes 1572864 | tf_op jit(solution)/shard_map/all_to_all | solution.py:143
  114.8 28.1 %collective-permute-start.4 = (bf16[512,1024]{1,0:T(8,128)(2,1)S(1)}, bf16[512,1024]{1,0:T(8,128)(2,1)S(1)}, u32[]{:S(2)}, u32[]{:S(2)}) collective-permute-start(bf16[512,1024]{1,0:T(8,128)(2,1)S(1)} %slice.164), channel_id=1, source_target_pairs={{0,8},{8,16},{16,24},{24,0},{1,9},{9,17},{17,25},{25,1},{2,10},{10... | collective-permute-start | bytes 3145736 | tf_op jit(solution)/shard_map/ppermute | solution.py:136
  118.9 46.4 %collective-permute-start.5 = (bf16[512,1024]{1,0:T(8,128)(2,1)S(1)}, bf16[512,1024]{1,0:T(8,128)(2,1)}, u32[]{:S(2)}, u32[]{:S(2)}) collective-permute-start(bf16[512,1024]{1,0:T(8,128)(2,1)S(1)} %slice.164), channel_id=1, source_target_pairs={{0,16},{8,24},{16,0},{24,8},{1,17},{9,25},{17,1},{25,9},{2,18},{10... | collective-permute-start | bytes 3145736 | tf_op jit(solution)/shard_map/ppermute | solution.py:136
  122.1 44.8 %collective-permute-start.6 = (bf16[512,1024]{1,0:T(8,128)(2,1)S(1)}, bf16[512,1024]{1,0:T(8,128)(2,1)}, u32[]{:S(2)}, u32[]{:S(2)}) collective-permute-start(bf16[512,1024]{1,0:T(8,128)(2,1)S(1)} %slice.164), channel_id=1, source_target_pairs={{0,24},{8,0},{16,8},{24,16},{1,25},{9,1},{17,9},{25,17},{2,26},{10... | collective-permute-start | bytes 3145736 | tf_op jit(solution)/shard_map/ppermute | solution.py:136
  171.1 5.5 %collective-permute-start.7 = (bf16[192,2048]{1,0:T(8,128)(2,1)S(1)}, bf16[192,2048]{1,0:T(8,128)(2,1)S(1)}, u32[]{:S(2)}, u32[]{:S(2)}) collective-permute-start(bf16[192,2048]{1,0:T(8,128)(2,1)S(1)} %get-tuple-element.68), channel_id=1, source_target_pairs={{0,1},{1,0},{2,3},{3,2},{4,5},{5,4},{6,7},{7,6},{8,9},{9,8},{10,11... | collective-permute-start | bytes 2359304 | tf_op jit(solution)/shard_map/ppermute | solution.py:212
